TPU v7x, 256 devices: a whole 4x4x8 slice. The times are simulated.
256 devices in a mesh: ep: 64 (over z, y, core), tp: 4 (over x).
Axes of the slice: x: 4, y: 4, z: 8, core: 2. Of those that a mesh axis runs over, the one named last changes fastest.
Arguments:
- resid: bfloat16 [2048, 2048], P('ep'), may hold values from -6 to 6
- mix_gain: bfloat16 [2048], replicated, may hold values from 0.099609375 to 1.8984375
- proj_x: bfloat16 [2048, 512], P(None, 'tp'), may hold values from -0.125 to 0.125
- proj_z: bfloat16 [2048, 512], P(None, 'tp'), may hold values from -0.125 to 0.125
- proj_b: bfloat16 [2048, 512], P(None, 'tp'), may hold values from -0.125 to 0.125
- proj_c: bfloat16 [2048, 512], P(None, 'tp'), may hold values from -0.125 to 0.125
- proj_step: bfloat16 [2048, 8], replicated, may hold values from -0.125 to 0.125
- step_bias: float32 [8], P('tp'), may hold values from -5 to -1
- decay_rate: float32 [8], P('tp'), may hold values from 1 to 16
- conv_taps: bfloat16 [3, 4, 512], P(None, None, 'tp'), may hold values from -3 to 3
- conv_state: bfloat16 [2048, 3, 3, 512], P('ep', None, None, 'tp'), may hold values from -6 to 6
- scan_state: float32 [2048, 8, 64, 128], P('ep', 'tp'), may hold values from -2.5 to 2.5
- inner_gain: bfloat16 [512], P('tp'), may hold values from 0.099609375 to 1.8984375
- proj_out: bfloat16 [512, 2048], P('tp'), may hold values from -0.25 to 0.25
- post_gain: bfloat16 [2048], replicated, may hold values from 0.099609375 to 1.8984375
- ffn_gain: bfloat16 [2048], replicated, may hold values from 0.099609375 to 1.8984375
- group_router: bfloat16 [2048, 2], replicated, may hold values from -0.125 to 0.125
- expert_router: bfloat16 [2048, 64], replicated, may hold values from -0.125 to 0.125
- route_experts: int32 [2048, 4], P('ep'), may hold values from 0 to 63, as said below
- expert_gate: bfloat16 [64, 2048, 1024], P('ep', None, 'tp'), may hold values from -0.125 to 0.125
- expert_up: bfloat16 [64, 2048, 1024], P('ep', None, 'tp'), may hold values from -0.125 to 0.125
- expert_down: bfloat16 [64, 1024, 2048], P('ep', 'tp')
- dense_switch: bfloat16 [2048], replicated, may hold values from -0.125 to 0.125
- dense_gate: bfloat16 [2048, 2048], P('ep', 'tp'), may hold values from -0.125 to 0.125
- dense_up: bfloat16 [2048, 2048], P('ep', 'tp'), may hold values from -0.125 to 0.125
- dense_down: bfloat16 [2048, 2048], P('ep', 'tp')
- out_gain: bfloat16 [2048], P('tp'), may hold values from 0.099609375 to 1.8984375
Outputs:
- layer_out: bfloat16 [2048, 2048], P('ep', 'tp')
- new_state: float32 [2048, 8, 64, 128], P('ep', 'tp')
- new_conv: bfloat16 [2048, 3, 3, 512], P('ep', None, None, 'tp')
Inputs may be any that keep to these rules, and one draw needn't show every extreme that they name: `route_experts`: each row names 4 different experts, all from one group of 32 consecutive expert numbers. Within each aligned block of 32 rows (the rows of one index of ep) no expert is named more than 4 times, and one expert, the same in every block, is named exactly 4 times in every block.
All inputs are finite; a program needn't handle non-finite values.
Results may differ from a plain program's by a relative error of at most 0.019.
Values may be sent and summed in bfloat16 or wider, within the bound.
A program may use at most 64 MiB of HBM per device.

v0:
```python
import jax
import jax.numpy as jnp
from jax import lax
from jax.sharding import Mesh
from jax.sharding import PartitionSpec as P

EP = ("ep_0", "ep_1", "ep_2")


norm_eps = 1e-06


def sent_to_all(array, axis):
    count = lax.axis_size(axis)
    return lax.all_to_all(
        jnp.broadcast_to(array[None], (count, *array.shape)), axis, 0, 0, tiled=True
    )


def taken_together(array, axis):
    return sent_to_all(array, axis).astype(jnp.float32).sum(axis=0)


def cut_along(array, dim, count):
    shape = array.shape
    pieces = array.reshape(*shape[:dim], count, shape[dim] // count, *shape[dim + 1 :])
    return jnp.moveaxis(pieces, dim, 0)


def sum_at_owner(array, axis, dim):
    count = lax.axis_size(axis)
    pieces = lax.all_to_all(cut_along(array, dim, count), axis, 0, 0, tiled=True)
    return jnp.sum(pieces.astype(jnp.float32), axis=0)


def laid_out(pieces, dim):
    shape = list(pieces.shape[1:])
    shape[dim] *= pieces.shape[0]
    return jnp.moveaxis(pieces, 0, dim).reshape(shape)


def exchange_in_order(pieces, axes, sequence):
    inside = pieces.shape[1:]
    result = pieces.reshape(*(lax.axis_size(a) for a in axes), *inside)
    for k in sequence:
        result = lax.all_to_all(result, axes[k], k, k, tiled=True)
    return result.reshape(-1, *inside)


def two_step_exchange(array, groups, sequence, split_dim, concat_dim):
    count = lax.axis_size(groups[0]) * lax.axis_size(groups[1])
    pieces = cut_along(array, split_dim, count)
    return laid_out(exchange_in_order(pieces, groups, sequence), concat_dim)


def gather_directly(array, axis, dim):
    return laid_out(sent_to_all(array, axis), dim)


def sent_together(arrays, axis, dim, along):
    widths = [a.shape[along] for a in arrays]
    both = jnp.concatenate(arrays, axis=along)
    result = lax.all_gather(both, axis, axis=dim, tiled=True)
    return tuple(jnp.split(result, [sum(widths[:k]) for k in range(1, len(widths))], axis=along))


def all_blocks(array, axes, sequence):
    pieces = array[None]
    for k in sequence:
        pieces = lax.all_gather(pieces, axes[k], axis=0, tiled=True)
    block = [lax.axis_size(axes[k]) for k in reversed(sequence)]
    pieces = pieces.reshape(*block, *array.shape)
    turned = sorted(range(len(sequence)), key=lambda place: sequence[len(sequence) - 1 - place])
    return pieces.transpose(*turned, *range(len(sequence), pieces.ndim)).reshape(-1, *array.shape)


def gathered_by_axis(array, axes, sequence, dim):
    return laid_out(all_blocks(array, axes, sequence), dim)


def taken_together_2(array, axis):
    return sent_to_all(array, axis).sum(axis=0)


def scaled_rows(values, gain):
    values = values.astype(jnp.float32)
    mean_square = jnp.mean(values * values, axis=-1, keepdims=True)
    return values * lax.rsqrt(mean_square + norm_eps) * gain.astype(jnp.float32)


def softmax_plain(logits):
    weights = jnp.exp(logits)
    return weights / jnp.sum(weights, axis=-1, keepdims=True)


def on_device(
    resid,
    mix_gain,
    proj_x,
    proj_z,
    proj_b,
    proj_c,
    proj_step,
    step_bias,
    decay_rate,
    conv_taps,
    conv_state,
    scan_state,
    inner_gain,
    proj_out,
    post_gain,
    ffn_gain,
    group_router,
    expert_router,
    route_experts,
    expert_gate,
    expert_up,
    expert_down,
    dense_switch,
    dense_gate,
    dense_up,
    dense_down,
    out_gain,
):
    tp_index = lax.axis_index("tp")
    seqs = resid.shape[0]
    width = resid.shape[1]
    quarter = width // lax.axis_size("tp")
    heads_here = scan_state.shape[1]
    head_dim = scan_state.shape[2]
    state_dim = scan_state.shape[3]
    channels = conv_state.shape[3]
    repeat = heads_here // (channels // state_dim)
    normed = scaled_rows(resid, mix_gain).astype(jnp.bfloat16)
    fresh = jnp.stack(
        [
            jnp.dot(normed, proj_x, preferred_element_type=jnp.float32),
            jnp.dot(normed, proj_b, preferred_element_type=jnp.float32),
            jnp.dot(normed, proj_c, preferred_element_type=jnp.float32),
        ],
        axis=1,
    ).astype(jnp.bfloat16)
    gate_z = jnp.dot(normed, proj_z, preferred_element_type=jnp.float32)
    step_all = jnp.dot(normed, proj_step, preferred_element_type=jnp.float32)
    step_raw = lax.dynamic_slice_in_dim(step_all, tp_index * heads_here, heads_here, 1)
    history = jnp.concatenate([conv_state, fresh[:, :, None, :]], axis=2)
    activated = jax.nn.silu(
        jnp.sum(history.astype(jnp.float32) * conv_taps.astype(jnp.float32)[None], axis=2)
    )
    xs_heads = activated[:, 0].reshape(seqs, heads_here, head_dim)
    b_heads = jnp.repeat(activated[:, 1].reshape(seqs, -1, state_dim), repeat, axis=1)
    c_heads = jnp.repeat(activated[:, 2].reshape(seqs, -1, state_dim), repeat, axis=1)
    step = jax.nn.softplus(step_raw + step_bias)
    keep = jnp.exp(-decay_rate * step)
    driven = step[:, :, None] * xs_heads
    new_state = keep[:, :, None, None] * scan_state + driven[:, :, :, None] * b_heads[:, :, None, :]
    read = jnp.sum(new_state * c_heads[:, :, None, :], axis=3).reshape(seqs, channels)
    gated = (read * jax.nn.silu(gate_z) * inner_gain.astype(jnp.float32)).astype(jnp.bfloat16)
    mixed = taken_together(
        jnp.dot(gated, proj_out, preferred_element_type=jnp.float32).astype(jnp.bfloat16), "tp"
    ).astype(jnp.float32)
    stream = (resid.astype(jnp.float32) + scaled_rows(mixed, post_gain)).astype(jnp.bfloat16)
    feed = scaled_rows(stream, ffn_gain).astype(jnp.bfloat16)
    feed_quarter = lax.dynamic_slice_in_dim(feed, tp_index * quarter, quarter, 1)
    expert_count = expert_router.shape[1]
    group_size = expert_count // group_router.shape[1]
    pick_count = route_experts.shape[1]
    group_prob = softmax_plain(jnp.dot(feed, group_router, preferred_element_type=jnp.float32))
    expert_logits = jnp.dot(feed, expert_router, preferred_element_type=jnp.float32)
    matches = route_experts[:, :, None] == jnp.arange(expert_count, dtype=jnp.int32)[None, None, :]
    pick_logits = jnp.sum(jnp.where(matches, expert_logits[:, None, :], 0.0), axis=2)
    chosen_group = route_experts[:, 0] // group_size
    group_ids = jnp.arange(group_router.shape[1], dtype=jnp.int32)
    group_weight = jnp.sum(
        jnp.where(chosen_group[:, None] == group_ids[None, :], group_prob, 0.0), axis=1
    )
    pick_weight = softmax_plain(pick_logits) * group_weight[:, None]
    capacity = 2 * seqs * pick_count // expert_count
    flat_picks = route_experts.reshape(-1)
    one_hot = (flat_picks[:, None] == jnp.arange(expert_count, dtype=jnp.int32)[None, :]).astype(
        jnp.int32
    )
    slot = jnp.sum((jnp.cumsum(one_hot, axis=0) - one_hot) * one_hot, axis=1)
    target = flat_picks * capacity + slot
    repeated = jnp.repeat(feed_quarter, pick_count, axis=0)
    outgoing = jnp.zeros((expert_count * capacity, quarter), jnp.bfloat16).at[target].set(repeated)
    outgoing = outgoing.reshape(expert_count, capacity, quarter)
    arrived = gather_directly(
        lax.all_to_all(outgoing, EP, split_axis=0, concat_axis=0, tiled=True), "tp", 2
    )
    sources = arrived.shape[0]
    items = arrived.shape[1]
    rows = arrived.reshape(sources * items, width)
    gate_value = jnp.dot(rows, expert_gate[0], preferred_element_type=jnp.float32)
    up_value = jnp.dot(rows, expert_up[0], preferred_element_type=jnp.float32)
    hidden = (jax.nn.silu(gate_value) * up_value).astype(jnp.bfloat16)
    result = jnp.dot(hidden, expert_down[0], preferred_element_type=jnp.float32).reshape(
        sources, items, width
    )
    summed = sum_at_owner(result.astype(jnp.bfloat16), "tp", 2)
    returned = two_step_exchange(
        summed.astype(jnp.bfloat16), (("ep_0", "ep_1"), "ep_2"), (1, 0), 0, 0
    )
    fetched = returned.reshape(expert_count * capacity, quarter)[target].reshape(
        seqs, pick_count, quarter
    )
    routed = jnp.sum(fetched.astype(jnp.float32) * pick_weight[:, :, None], axis=1)
    pieces = sent_together((dense_gate, dense_up), EP, 0, 1)
    gate_piece = jnp.einsum(
        "sd,cd->sc", feed_quarter, pieces[0], preferred_element_type=jnp.float32
    )
    up_piece = jnp.einsum("sd,cd->sc", feed_quarter, pieces[1], preferred_element_type=jnp.float32)
    gate_sum = gate_piece
    up_sum = up_piece
    gate_sum, up_sum = (
        taken_together(gate_sum.astype(jnp.bfloat16), "tp").astype(jnp.float32),
        taken_together(up_sum.astype(jnp.bfloat16), "tp").astype(jnp.float32),
    )
    dense_hidden = (jax.nn.silu(gate_sum) * up_sum).astype(jnp.bfloat16)
    dense_out = jnp.dot(
        dense_hidden,
        gathered_by_axis(dense_down, EP, (1, 0, 2), 0),
        preferred_element_type=jnp.float32,
    )
    switch = jax.nn.sigmoid(jnp.dot(feed, dense_switch, preferred_element_type=jnp.float32))
    combined = routed + switch[:, None] * dense_out
    total_square = taken_together_2(jnp.sum(combined * combined, axis=1), "tp")
    scale = lax.rsqrt(total_square / width + norm_eps)
    stream_part = lax.dynamic_slice_in_dim(stream, tp_index * quarter, quarter, 1).astype(
        jnp.float32
    )
    layer_out = (stream_part + combined * scale[:, None] * out_gain.astype(jnp.float32)).astype(
        jnp.bfloat16
    )
    new_conv = history[:, :, 1:, :]
    return (layer_out, new_state, new_conv)


def solution(mesh):
    torus = Mesh(mesh.devices.reshape(8, 4, 2, mesh.shape["tp"]), ("ep_0", "ep_1", "ep_2", "tp"))
    in_specs = (
        P(EP, None),
        P(),
        P(None, "tp"),
        P(None, "tp"),
        P(None, "tp"),
        P(None, "tp"),
        P(),
        P("tp"),
        P("tp"),
        P(None, None, "tp"),
        P(EP, None, None, "tp"),
        P(EP, "tp", None, None),
        P("tp"),
        P("tp", None),
        P(),
        P(),
        P(),
        P(),
        P(EP, None),
        P(EP, None, "tp"),
        P(EP, None, "tp"),
        P(EP, "tp", None),
        P(),
        P(EP, "tp"),
        P(EP, "tp"),
        P(EP, "tp"),
        P("tp"),
    )
    out_specs = (P(EP, "tp"), P(EP, "tp", None, None), P(EP, None, None, "tp"))
    return jax.shard_map(
        on_device, mesh=torus, in_specs=in_specs, out_specs=out_specs, check_vma=False
    )
```

profile of v0, /device:TPU:8, one launch (start us, length us, event | category | flops | bytes accessed | tf_op | source)
XLA Modules:
  0.0 194.9 jit_solution(9819140083257767766)
XLA Ops:
  7.3 13.5 %all-gather = bf16[128,512]{1,0:T(8,128)(2,1)} all-gather(bf16[32,512]{1,0:T(8,128)(2,1)} %param.52), channel_id=2, replica_groups=mesh['ep_0'=8,'ep_1'=4,'ep_2'=2,'tp'=4] {'ep_1'}, dimensions={0}, use_global_device_ids=true | all-gather | bytes 163840 | tf_op jit(solution)/shard_map/all_gather | solution.py:70
  20.8 1.4 pad_maximum_fusion
  24.7 1.4 fusion.4
  26.1 1.4 fusion.5
  27.5 1.4 fusion.6
  30.3 2.1 %multiply_reduce_fusion = (f32[32,2,64]{2,1,0:T(2,128)S(1)}, f32[32,2,64,128]{3,2,1,0:T(8,128)}) fusion(f32[32,128]{1,0:T(8,128)S(1)} %get-tuple-element.12, f32[32,128]{1,0:T(8,128)S(1)} %get-tuple-element.13, f32[32,2,64]{2,1,0:T(2,128)S(1)} %broadcast_multiply_fusion, f32[32,2,64,128]{3,2,1,0:T(8,128)S(1)} %copy-done.2, f32[32,2]{1,0:T(8,128)S(1)} %copy.73), kind=kLoop, calls=%fused_computation.8 | loop fusion | flops 2617344 | bytes 4260096 | tf_op jit(solution)/shard_map/reduce_sum | solution.py:157
  32.6 1.7 convolution_convert_fusion.3
  35.1 4.1 %all-to-all-start = ((bf16[4,32,2048]{2,1,0:T(8,128)(2,1)}), bf16[4,32,2048]{2,1,0:T(8,128)(2,1)S(1)}, u32[]{:S(2)}, u32[]{:S(2)}) async-start(bf16[4,32,2048]{2,1,0:T(8,128)(2,1)} %broadcast_in_dim.25), calls=%async_computation | async-start | bytes 1048576 | tf_op jit(solution)/shard_map/all_to_all | solution.py:15
  40.1 7.2 %all-to-all-done = bf16[4,32,2048]{2,1,0:T(8,128)(2,1)S(1)} async-done(((bf16[4,32,2048]{2,1,0:T(8,128)(2,1)}), bf16[4,32,2048]{2,1,0:T(8,128)(2,1)S(1)}, u32[]{:S(2)}, u32[]{:S(2)}) %all-to-all-start) | async-done | bytes 524320 | tf_op jit(solution)/shard_map/all_to_all | solution.py:15
  48.0 1.1 scatter_custom_fusion
  49.2 23.7 %all_to_all.46 = bf16[64,4,512]{2,1,0:T(4,128)(2,1)S(1)} all-to-all(bf16[64,4,512]{2,1,0:T(4,128)(2,1)S(1)} %reshape.201), channel_id=1, replica_groups=mesh['ep_0'=8,'ep_1'=4,'ep_2'=2,'tp'=4] {'ep_0','ep_1','ep_2'}, dimensions={0} | all-to-all | bytes 524288 | tf_op jit(solution)/shard_map/all_to_all | solution.py:189
  73.2 18.1 %all_to_all.47 = bf16[4,64,4,512]{3,2,1,0:T(4,128)(2,1)S(1)} all-to-all(bf16[4,64,4,512]{3,2,1,0:T(4,128)(2,1)S(1)} %broadcast_in_dim.28), channel_id=1, replica_groups=mesh['ep_0'=8,'ep_1'=4,'ep_2'=2,'tp'=4] {'tp'}, dimensions={0} | all-to-all | bytes 2097152 | tf_op jit(solution)/shard_map/all_to_all | solution.py:15
  91.3 1.4 copy.77
  94.8 1.1 copy.92
  95.9 3.6 %all-to-all-start.3 = ((bf16[4,64,4,512]{3,1,2,0:T(8,128)(2,1)}), bf16[4,64,4,512]{3,1,2,0:T(8,128)(2,1)S(1)}, u32[]{:S(2)}, u32[]{:S(2)}) async-start(bf16[4,64,4,512]{3,1,2,0:T(8,128)(2,1)} %bitcast.77), calls=%async_computation.3 | async-start | bytes 2097152 | tf_op jit(solution)/shard_map/all_to_all | solution.py:32
  100.8 13.6 %all-to-all-done.3 = bf16[4,64,4,512]{3,1,2,0:T(8,128)(2,1)S(1)} async-done(((bf16[4,64,4,512]{3,1,2,0:T(8,128)(2,1)}), bf16[4,64,4,512]{3,1,2,0:T(8,128)(2,1)S(1)}, u32[]{:S(2)}, u32[]{:S(2)}) %all-to-all-start.3) | async-done | bytes 1048608 | tf_op jit(solution)/shard_map/all_to_all | solution.py:32
  114.9 4.0 %all_to_all.48 = bf16[32,2,1,4,512]{4,3,0,2,1:T(4,128)(2,1)S(1)} all-to-all(bf16[32,2,1,4,512]{4,3,0,2,1:T(4,128)(2,1)S(1)} %copy.81), channel_id=1, replica_groups=mesh['ep_0'=8,'ep_1'=4,'ep_2'=2,'tp'=4] {'ep_2'}, dimensions={1} | all-to-all | bytes 524288 | tf_op jit(solution)/shard_map/all_to_all | solution.py:46
  119.7 5.0 %all-to-all-start.5 = ((bf16[32,2,1,4,512]{4,3,1,2,0:T(4,128)(2,1)}), bf16[32,2,1,4,512]{4,3,1,2,0:T(4,128)(2,1)S(1)}, u32[]{:S(2)}, u32[]{:S(2)}) async-start(bf16[32,2,1,4,512]{4,3,1,2,0:T(4,128)(2,1)} %copy.82), calls=%async_computation.5 | async-start | bytes 524288 | tf_op jit(solution)/shard_map/all_to_all | solution.py:46
  125.0 18.5 %all-gather.5.cloned.1.call-done = bf16[2048,1024]{1,0:T(8,128)(2,1)} async-done(((bf16[32,1024]{1,0:T(8,128)(2,1)}), bf16[2048,1024]{1,0:T(8,128)(2,1)}) %all-gather.5.cloned.1.call-update) | async-done | bytes 4194320 | tf_op jit(solution)/shard_map/all_gather | solution.py:63
  143.5 2.3 %convolution_convert_fusion.1 = bf16[32,2048]{1,0:T(8,128)(2,1)S(1)} fusion(bf16[32,512]{1,0:T(8,128)(2,1)S(1)} %constant_dynamic-slice_fusion, bf16[2048,1024]{1,0:T(8,128)(2,1)} %all-gather.5.cloned.1.call-done), kind=kOutput, calls=%fused_computation.3 | convolution fusion | flops 67174400 | bytes 2260992 | tf_op jit(solution)/shard_map/sd,cd->sc/dot_general | solution.py:212
  146.6 4.1 %all-to-all-start.7 = ((bf16[4,32,2048]{2,1,0:T(8,128)(2,1)}), bf16[4,32,2048]{2,1,0:T(8,128)(2,1)S(1)}, u32[]{:S(2)}, u32[]{:S(2)}) async-start(bf16[4,32,2048]{2,1,0:T(8,128)(2,1)} %broadcast_in_dim.37), calls=%async_computation.7 | async-start | bytes 1048576 | tf_op jit(solution)/shard_map/all_to_all | solution.py:15
  150.8 2.3 %convolution_convert_fusion.2 = bf16[32,2048]{1,0:T(8,128)(2,1)S(1)} fusion(bf16[32,512]{1,0:T(8,128)(2,1)S(1)} %constant_dynamic-slice_fusion, bf16[2048,1024]{1,0:T(8,128)(2,1)} %all-gather.5.cloned.1.call-done), kind=kOutput, calls=%fused_computation.4 | convolution fusion | flops 67174400 | bytes 2260992 | tf_op jit(solution)/shard_map/sd,cd->sc/dot_general | solution.py:209
  153.1 7.5 %all-to-all-done.7 = bf16[4,32,2048]{2,1,0:T(8,128)(2,1)S(1)} async-done(((bf16[4,32,2048]{2,1,0:T(8,128)(2,1)}), bf16[4,32,2048]{2,1,0:T(8,128)(2,1)S(1)}, u32[]{:S(2)}, u32[]{:S(2)}) %all-to-all-start.7) | async-done | bytes 524320 | tf_op jit(solution)/shard_map/all_to_all | solution.py:15
  161.5 4.1 %all-to-all-start.6 = ((bf16[4,32,2048]{2,1,0:T(8,128)(2,1)}), bf16[4,32,2048]{2,1,0:T(8,128)(2,1)}, u32[]{:S(2)}, u32[]{:S(2)}) async-start(bf16[4,32,2048]{2,1,0:T(8,128)(2,1)} %broadcast_in_dim.35), calls=%async_computation.6 | async-start | bytes 1048576 | tf_op jit(solution)/shard_map/all_to_all | solution.py:15
  167.7 1.8 copy.84
  169.6 5.1 %all-to-all-done.6 = bf16[4,32,2048]{2,1,0:T(8,128)(2,1)} async-done(((bf16[4,32,2048]{2,1,0:T(8,128)(2,1)}), bf16[4,32,2048]{2,1,0:T(8,128)(2,1)}, u32[]{:S(2)}, u32[]{:S(2)}) %all-to-all-start.6) | async-done | bytes 524320 | tf_op jit(solution)/shard_map/all_to_all | solution.py:15
  174.7 1.1 convert_reduce_fusion.1
  175.9 2.0 %multiply_reduce_fusion.4 = (f32[32]{0:T(128)S(1)}, f32[32,512]{1,0:T(8,128)}) fusion(f32[32,512]{1,0:T(8,128)} %multiply_reduce_fusion.1, bf16[2048,512]{1,0:T(8,128)(2,1)S(1)} %bitcast.78, f32[32,2048]{1,0:T(8,128)S(1)} %convert_reduce_fusion, f32[32,2048]{1,0:T(8,128)S(1)} %convert_reduce_fusion.1, f32[32]{0:T(128)S(1)} %fusion.10), kind=kOutput, calls=%fused_computation.57 | convolution fusion | flops 67567584 | bytes 2752768 | tf_op jit(solution)/shard_map/dot_general | solution.py:220
  178.4 3.2 %all-to-all-start.8 = ((f32[4,1,32]{2,1,0:T(1,128)}), f32[4,1,32]{2,1,0:T(1,128)S(1)}, u32[]{:S(2)}, u32[]{:S(2)}) async-start(f32[4,1,32]{2,1,0:T(1,128)} %broadcast_in_dim.39), calls=%async_computation.8 | async-start | bytes 4096 | tf_op jit(solution)/shard_map/all_to_all | solution.py:15
  181.7 1.5 slice.31
  183.2 3.6 %all-to-all-done.8 = f32[4,1,32]{2,1,0:T(1,128)S(1)} async-done(((f32[4,1,32]{2,1,0:T(1,128)}), f32[4,1,32]{2,1,0:T(1,128)S(1)}, u32[]{:S(2)}, u32[]{:S(2)}) %all-to-all-start.8) | async-done | bytes 544 | tf_op jit(solution)/shard_map/all_to_all | solution.py:15
  186.9 1.5 add_convert_fusion
  (117 shorter events, 16.1 us)
Async XLA Ops:
  7.2 87.2 %copy-start = (bf16[1,256,2048]{2,1,0:T(8,128)(2,1)S(1)}, bf16[1,256,2048]{2,1,0:T(8,128)(2,1)}, u32[]{:S(2)}) copy-start(bf16[1,256,2048]{2,1,0:T(8,128)(2,1)} %param.48) | copy-start | bytes 3145732
  7.2 22.5 %copy-start.1 = (bf16[32,2048]{1,0:T(8,128)(2,1)S(1)}, bf16[32,2048]{1,0:T(8,128)(2,1)}, u32[]{:S(2)}) copy-start(bf16[32,2048]{1,0:T(8,128)(2,1)} %param.27) | copy-start | bytes 393220
  7.2 21.7 %copy-start.7 = (bf16[32,3,3,128]{3,0,2,1:T(8,128)(2,1)S(1)}, bf16[32,3,3,128]{3,0,2,1:T(8,128)(2,1)}, u32[]{:S(2)}) copy-start(bf16[32,3,3,128]{3,0,2,1:T(8,128)(2,1)} %param.37) | copy-start | bytes 221188
  7.2 22.5 %copy-start.17 = (f32[2]{0:T(128)S(1)}, f32[2]{0:T(128)}, u32[]{:S(2)}) copy-start(f32[2]{0:T(128)} %param.35) | copy-start | bytes 28
  7.2 22.5 %copy-start.15 = (bf16[2048,8]{0,1:T(8,128)(2,1)S(1)}, bf16[2048,8]{0,1:T(8,128)(2,1)}, u32[]{:S(2)}) copy-start(bf16[2048,8]{0,1:T(8,128)(2,1)} %param.33) | copy-start | bytes 98308
  7.2 22.7 %copy-start.13 = (f32[2]{0:T(128)S(1)}, f32[2]{0:T(128)}, u32[]{:S(2)}) copy-start(f32[2]{0:T(128)} %param.34) | copy-start | bytes 28
  7.2 23.1 %copy-start.2 = (f32[32,2,64,128]{3,2,1,0:T(8,128)S(1)}, f32[32,2,64,128]{3,2,1,0:T(8,128)}, u32[]{:S(2)}) copy-start(f32[32,2,64,128]{3,2,1,0:T(8,128)} %param.38) | copy-start | bytes 6291460
  7.2 92.4 %all-gather.7.cloned.1.call-start = ((), (), s32[]{:S(2)}) async-start(), calls=%async_computation.10 | async-start | bytes 1179648 | tf_op jit(solution)/shard_map/all_gather | solution.py:70
  20.8 122.7 %all-gather.5.cloned.1.call-start = ((), (), s32[]{:S(2)}) async-start(), calls=%async_computation.9 | async-start | bytes 4259840 | tf_op jit(solution)/shard_map/all_gather | solution.py:63
  30.3 2.3 %copy-start.18 = (bf16[128]{0:T(256)(128)(2,1)S(1)}, bf16[128]{0:T(256)(128)(2,1)}, u32[]{:S(2)}) copy-start(bf16[128]{0:T(256)(128)(2,1)} %param.39) | copy-start | bytes 772
  32.5 6.8 %copy-start.8 = (s32[32,4]{0,1:T(4,128)S(1)}, s32[32,4]{0,1:T(4,128)}, u32[]{:S(2)}) copy-start(s32[32,4]{0,1:T(4,128)} %param.45) | copy-start | bytes 1540
  32.5 7.1 %copy-start.9 = (bf16[2048]{0:T(1024)(128)(2,1)S(1)}, bf16[2048]{0:T(1024)(128)(2,1)}, u32[]{:S(2)}) copy-start(bf16[2048]{0:T(1024)(128)(2,1)} %param.41) | copy-start | bytes 12292
  32.5 7.1 %copy-start.10 = (bf16[2048]{0:T(1024)(128)(2,1)S(1)}, bf16[2048]{0:T(1024)(128)(2,1)}, u32[]{:S(2)}) copy-start(bf16[2048]{0:T(1024)(128)(2,1)} %param.42) | copy-start | bytes 12292
  35.1 12.2 %all-to-all-start = ((bf16[4,32,2048]{2,1,0:T(8,128)(2,1)}), bf16[4,32,2048]{2,1,0:T(8,128)(2,1)S(1)}, u32[]{:S(2)}, u32[]{:S(2)}) async-start(bf16[4,32,2048]{2,1,0:T(8,128)(2,1)} %broadcast_in_dim.25), calls=%async_computation | async-start | bytes 1048576 | tf_op jit(solution)/shard_map/all_to_all | solution.py:15
  91.3 1.6 copy-start.5
  92.7 1.2 copy-start.14
  95.9 4.4 %copy-start.11 = (bf16[2048]{0:T(1024)(128)(2,1)S(1)}, bf16[2048]{0:T(1024)(128)(2,1)}, u32[]{:S(2)}) copy-start(bf16[2048]{0:T(1024)(128)(2,1)} %param.49) | copy-start | bytes 12292
  95.9 4.5 %copy-start.16 = (bf16[2048,2]{0,1:T(2,128)(2,1)S(1)}, bf16[2048,2]{0,1:T(2,128)(2,1)}, u32[]{:S(2)}) copy-start(bf16[2048,2]{0,1:T(2,128)(2,1)} %param.43) | copy-start | bytes 24580
  95.9 4.6 %copy-start.6 = (bf16[2048,64]{0,1:T(8,128)(2,1)S(1)}, bf16[2048,64]{0,1:T(8,128)(2,1)}, u32[]{:S(2)}) copy-start(bf16[2048,64]{0,1:T(8,128)(2,1)} %param.44) | copy-start | bytes 786436
  95.9 18.5 %all-to-all-start.3 = ((bf16[4,64,4,512]{3,1,2,0:T(8,128)(2,1)}), bf16[4,64,4,512]{3,1,2,0:T(8,128)(2,1)S(1)}, u32[]{:S(2)}, u32[]{:S(2)}) async-start(bf16[4,64,4,512]{3,1,2,0:T(8,128)(2,1)} %bitcast.77), calls=%async_computation.3 | async-start | bytes 2097152 | tf_op jit(solution)/shard_map/all_to_all | solution.py:32
  99.6 68.1 %all-gather.9.cloned.1.call-start = ((), (), s32[]{:S(2)}) async-start(), calls=%async_computation.11 | async-start | bytes 3145728 | tf_op jit(solution)/shard_map/all_gather | solution.py:70
  119.7 26.0 %all-to-all-start.5 = ((bf16[32,2,1,4,512]{4,3,1,2,0:T(4,128)(2,1)}), bf16[32,2,1,4,512]{4,3,1,2,0:T(4,128)(2,1)S(1)}, u32[]{:S(2)}, u32[]{:S(2)}) async-start(bf16[32,2,1,4,512]{4,3,1,2,0:T(4,128)(2,1)} %copy.82), calls=%async_computation.5 | async-start | bytes 524288 | tf_op jit(solution)/shard_map/all_to_all | solution.py:46
  146.6 13.9 %all-to-all-start.7 = ((bf16[4,32,2048]{2,1,0:T(8,128)(2,1)}), bf16[4,32,2048]{2,1,0:T(8,128)(2,1)S(1)}, u32[]{:S(2)}, u32[]{:S(2)}) async-start(bf16[4,32,2048]{2,1,0:T(8,128)(2,1)} %broadcast_in_dim.37), calls=%async_computation.7 | async-start | bytes 1048576 | tf_op jit(solution)/shard_map/all_to_all | solution.py:15
  160.6 5.1 %copy-start.3 = (bf16[4,32,2048]{2,1,0:T(8,128)(2,1)}, bf16[4,32,2048]{2,1,0:T(8,128)(2,1)S(1)}, u32[]{:S(2)}) copy-start(bf16[4,32,2048]{2,1,0:T(8,128)(2,1)S(1)} %all-to-all-done.7) | copy-start | bytes 1572868
  161.5 13.2 %all-to-all-start.6 = ((bf16[4,32,2048]{2,1,0:T(8,128)(2,1)}), bf16[4,32,2048]{2,1,0:T(8,128)(2,1)}, u32[]{:S(2)}, u32[]{:S(2)}) async-start(bf16[4,32,2048]{2,1,0:T(8,128)(2,1)} %broadcast_in_dim.35), calls=%async_computation.6 | async-start | bytes 1048576 | tf_op jit(solution)/shard_map/all_to_all | solution.py:15
  167.7 1.8 copy-start.4
  169.5 12.2 %copy-start.12 = (bf16[512]{0:T(512)(128)(2,1)S(1)}, bf16[512]{0:T(512)(128)(2,1)}, u32[]{:S(2)}) copy-start(bf16[512]{0:T(512)(128)(2,1)} %param.53) | copy-start | bytes 3076
  178.4 8.4 %all-to-all-start.8 = ((f32[4,1,32]{2,1,0:T(1,128)}), f32[4,1,32]{2,1,0:T(1,128)S(1)}, u32[]{:S(2)}, u32[]{:S(2)}) async-start(f32[4,1,32]{2,1,0:T(1,128)} %broadcast_in_dim.39), calls=%async_computation.8 | async-start | bytes 4096 | tf_op jit(solution)/shard_map/all_to_all | solution.py:15
Sparse Core Ops, SparseCore 0:
  20.9 40.6 all-gather.6
  65.0 78.4 all-gather.4
  145.3 14.7 all-gather.8
where the time goes:
time: 197 us; the launch traced here: 195 us
  blocking collectives  59.3 us (30%)
  waiting for transfers between devices  56.2 us (29%)
  starting transfers between devices  24.3 us (12%)
  local copies, waits for them, and re-layouts  14.4 us (7%)
  matrix products  14.4 us (7%)
  between operations  14.3 us (7%)
  other arithmetic  12 us (6%)
    all_to_all x1, blocking collectives, on_device(): lax.all_to_all(outgoing, EP, split_axis=0, concat_axis=0, tiled=True)  23.7 us
    all_to_all x4, waiting for transfers between devices, sent_to_all(): lax.all_to_all(jnp.broadcast_to(array[None], (count, *array.shape)), axis...  23.4 us
    all_gather x1, waiting for transfers between devices, sent_together(): result = lax.all_gather(both, axis, axis=dim, tiled=True)  18.5 us
    all_to_all x1, blocking collectives, sent_to_all(): lax.all_to_all(jnp.broadcast_to(array[None], (count, *array.shape)), axis...  18.1 us
    all_to_all x4, starting transfers between devices, sent_to_all(): lax.all_to_all(jnp.broadcast_to(array[None], (count, *array.shape)), axis...  15.5 us
    all_to_all x1, waiting for transfers between devices, sum_at_owner(): lax.all_to_all(cut_along(array, dim, count), axis, 0, 0, tiled=True)  13.6 us
    all_gather x1, blocking collectives, all_blocks(): pieces = lax.all_gather(pieces, axes[k], axis=0, tiled=True)  13.5 us
    all_to_all x1, starting transfers between devices, exchange_in_order(): result = lax.all_to_all(result, axes[k], k, k, tiled=True)  5.03 us
  transfers between devices with their start and end apart: 9, of which 6 were waited for; matrix products, arithmetic and copies ran while one was open for 18% of the time, Pallas kernels for 0%

commit v1 on v0

v1 whole, which is shorter than its diff:
```python
import functools

import jax
import jax.numpy as jnp
from jax import lax
from jax.experimental import pallas as pl
from jax.experimental.pallas import tpu as pltpu
from jax.sharding import Mesh
from jax.sharding import PartitionSpec as P

EP = ("ep_0", "ep_1", "ep_2")
MESH = pl.DeviceIdType.MESH
norm_eps = 1e-06
CAPACITY = 4
LANES = 128


def dot(a, b):
    return jnp.dot(a, b, preferred_element_type=jnp.float32)


def dot_nt(a, b):
    return lax.dot_general(a, b, (((1,), (1,)), ((), ())), preferred_element_type=jnp.float32)


def in_row(gain_ref):
    gain = gain_ref[...].astype(jnp.float32)
    return jnp.concatenate([gain[i : i + 1] for i in range(gain.shape[0])], axis=1)


def iota(shape, dim):
    return lax.broadcasted_iota(jnp.int32, shape, dim)


def shift_of(count):
    return count.bit_length() - 1


def root_mean(values):
    return values * lax.rsqrt(jnp.mean(values * values, axis=-1, keepdims=True) + norm_eps)


def rest_of_layer(
    sizes,
    gated,
    proj_out,
    resid,
    post_gain,
    ffn_gain,
    switch_row,
    group_rows,
    expert_rows,
    route,
    expert_gate,
    expert_up,
    expert_down,
    dense_gate,
    dense_up,
    dense_down,
    out_gain,
    layer_out,
    w_gate,
    w_up,
    w_down,
    d_gate,
    d_up,
    d_down,
    mixed_f,
    mixed_b,
    mixed_in,
    feed_out,
    feed_in,
    stream_out,
    stream_in,
    pick_in,
    pick_z,
    code_z,
    feed_z,
    rows_out,
    rows_in,
    rows_x,
    pre_out,
    pre_in,
    hidden_x,
    sum_out,
    sum_in,
    back_out,
    back_in,
    last_out,
    last_in,
    square_x,
    send_sem,
    recv_sem,
    local_sem,
):
    nz, ny, nc, nx, cap = sizes
    np_ = ny * nc
    z, y, c, x = (lax.axis_index(a) for a in ("ep_0", "ep_1", "ep_2", "tp"))
    place = y * nc + c
    toks = gated.shape[0]
    own = toks // nx
    width = proj_out.shape[1]
    quarter = width // nx
    all_toks = nz * toks
    rows = np_ * nz * cap
    half = np_ // 2

    def z_dev(r):
        return {"ep_0": lax.rem(z + r, nz)}

    def p_dev(q):
        to = lax.rem(place + q, np_)
        return {"ep_1": to // nc, "ep_2": lax.rem(to, nc)}

    def x_dev(r):
        return {"tp": lax.rem(x + r, nx)}

    used = [0]
    started = []

    def send(src, dst, device):
        k = used[0]
        used[0] += 1
        copy = pltpu.make_async_remote_copy(
            src_ref=src,
            dst_ref=dst,
            send_sem=send_sem.at[k],
            recv_sem=recv_sem.at[k],
            device_id=device,
            device_id_type=MESH,
        )
        copy.start()
        started.append(copy)
        return copy

    local = []

    def fetch(src, dst):
        copy = pltpu.make_async_copy(src, dst, local_sem.at[len(local)])
        copy.start()
        local.append(copy)
        return copy

    def arrive(copies):
        for copy in copies:
            copy.wait_recv()

    barrier = pltpu.get_barrier_semaphore()
    peers = (
        [x_dev(r) for r in range(1, nx)]
        + [p_dev(q) for q in range(1, np_)]
        + [z_dev(r) for r in range(1, nz)]
    )
    for device in peers:
        pl.semaphore_signal(barrier, inc=1, device_id=device, device_id_type=MESH)

    own_dense = [
        fetch(dense_gate, d_gate.at[0]),
        fetch(dense_up, d_up.at[0]),
        fetch(dense_down, d_down.at[0]),
    ]
    own_expert = [fetch(expert_gate, w_gate), fetch(expert_up, w_up)]
    own_expert += [
        fetch(expert_down.at[:, pl.ds(j * quarter, quarter)], w_down.at[j]) for j in range(nx)
    ]

    route_t = route[...]
    picks = route_t.shape[0]
    expert_ids = iota((LANES, toks), 0)
    named = jnp.zeros((LANES, toks), jnp.float32)
    for k in range(picks):
        named += jnp.where(expert_ids == route_t[k : k + 1, :], 1.0, 0.0)
    named_b = named.astype(jnp.bfloat16)
    before = jnp.where(iota((toks, toks), 0) < iota((toks, toks), 1), 1.0, 0.0).astype(jnp.bfloat16)
    code_t = (named * (dot(named_b, before) + 1.0)).astype(jnp.bfloat16)
    eye = jnp.where(iota((toks, toks), 0) == iota((toks, toks), 1), 1.0, 0.0).astype(jnp.bfloat16)
    code_z[0] = dot_nt(eye, code_t).astype(jnp.bfloat16)

    share = dot(gated[...], proj_out[...]).reshape(nx, own, width)
    mixed_f[...] = share
    mixed_b[...] = share.astype(jnp.bfloat16)

    pl.semaphore_wait(barrier, len(peers))

    copies = [
        send(mixed_b.at[lax.rem(x + r, nx)], mixed_in.at[r - 1], x_dev(r)) for r in range(1, nx)
    ]
    code_copies = [send(code_z.at[0], code_z.at[r], z_dev(r)) for r in range(1, nz)]
    dense_copies = []
    for src, dst in ((dense_gate, d_gate), (dense_up, d_up), (dense_down, d_down)):
        dense_copies += [send(src, dst.at[q], p_dev(q)) for q in range(1, np_)]

    arrive(copies)
    mixed = mixed_f[x]
    for r in range(1, nx):
        mixed += mixed_in[r - 1].astype(jnp.float32)
    stream = (resid[x].astype(jnp.float32) + root_mean(mixed) * in_row(post_gain)).astype(
        jnp.bfloat16
    )
    feed = (root_mean(stream.astype(jnp.float32)) * in_row(ffn_gain)).astype(jnp.bfloat16)
    for j in range(nx):
        feed_out[j] = feed[:, j * quarter : (j + 1) * quarter]
        stream_out[j] = stream[:, j * quarter : (j + 1) * quarter]
    feed_in[x] = feed_out[x]
    feed_copies = [
        send(feed_out.at[lax.rem(x + r, nx)], feed_in.at[x], x_dev(r)) for r in range(1, nx)
    ]

    feed_f = feed.astype(jnp.float32)
    experts = expert_rows.shape[0]
    groups = group_rows.shape[0]
    group_size = experts // groups
    token_pick = jnp.where(iota((own, toks), 1) == iota((own, toks), 0) + x * own, 1.0, 0.0)
    own_route = dot_nt(token_pick.astype(jnp.bfloat16), route_t.astype(jnp.bfloat16))
    logits = dot_nt(feed, expert_rows[...])
    lanes = iota((own, experts), 1).astype(jnp.float32)
    weights = []
    for k in range(picks):
        chosen = jnp.sum(
            jnp.where(lanes == own_route[:, k : k + 1], logits, 0.0), axis=1, keepdims=True
        )
        weights.append(jnp.exp(chosen))
    total = functools.reduce(jnp.add, weights)
    group_f = group_rows[...].astype(jnp.float32)
    group_exp = [
        jnp.exp(jnp.sum(feed_f * group_f[g : g + 1], axis=1, keepdims=True)) for g in range(groups)
    ]
    group_total = functools.reduce(jnp.add, group_exp)
    first = own_route[:, 0:1]
    group_weight = jnp.zeros((own, 1), jnp.float32)
    for g in range(groups):
        here = (first >= g * group_size) & (first < (g + 1) * group_size)
        group_weight += jnp.where(here, group_exp[g] / group_total, 0.0)
    switch = jax.nn.sigmoid(jnp.sum(feed_f * in_row(switch_row), axis=1, keepdims=True))
    all_lanes = iota((own, LANES), 1).astype(jnp.float32)
    pick_table = jnp.where(all_lanes < experts, 0.0, switch)
    for k in range(picks):
        pick_table += jnp.where(
            all_lanes == own_route[:, k : k + 1], weights[k] / total * group_weight, 0.0
        )
    pick_in[x] = pick_table

    arrive(feed_copies)
    feed_z[0] = feed_in[...].astype(jnp.float32).reshape(toks, quarter).astype(jnp.bfloat16)
    feed_copies = [send(feed_z.at[0], feed_z.at[r], z_dev(r)) for r in range(1, nz)]
    pick_copies = [send(pick_in.at[x], pick_in.at[x], x_dev(r)) for r in range(1, nx)]
    stream_in[x] = stream_out[x]
    stream_copies = [
        send(stream_out.at[lax.rem(x + r, nx)], stream_in.at[x], x_dev(r)) for r in range(1, nx)
    ]

    arrive(code_copies)
    codes = code_z[...].reshape(all_toks, LANES)
    step = shift_of(nz * cap)

    def expert_of(j):
        return z * np_ + ((place + (j >> step)) & (np_ - 1))

    def block_of(j):
        return (j & (nz * cap - 1)) >> shift_of(cap)

    def slot_of(j):
        return ((j & (cap - 1)) + 1).astype(jnp.float32)

    choose_t = jnp.where(
        iota((rows, LANES), 1) == expert_of(iota((rows, LANES), 0)), 1.0, 0.0
    ).astype(jnp.bfloat16)
    choose = jnp.where(
        iota((LANES, rows), 0) == expert_of(iota((LANES, rows), 1)), 1.0, 0.0
    ).astype(jnp.bfloat16)
    j_row = iota((rows, all_toks), 0)
    t_col = iota((rows, all_toks), 1)
    put = jnp.where(
        (dot_nt(choose_t, codes) == slot_of(j_row)) & (block_of(j_row) == t_col >> shift_of(toks)),
        1.0,
        0.0,
    ).astype(jnp.bfloat16)

    arrive(pick_copies)
    pick_z[0] = pick_in[...].reshape(toks, LANES)
    pick_copies = [send(pick_z.at[0], pick_z.at[r], z_dev(r)) for r in range(1, nz)]

    arrive(feed_copies)
    feeds = feed_z[...].reshape(all_toks, quarter)
    rows_out[...] = dot(put, feeds).astype(jnp.bfloat16).reshape(rows_out.shape)
    rows_in[0] = rows_out[0]
    row_copies = [None] + [send(rows_out.at[q], rows_in.at[q], p_dev(q)) for q in range(1, np_)]

    for copy in own_dense:
        copy.wait()
    arrive(dense_copies)
    hidden_here = d_gate.shape[0] * d_gate.shape[1]
    for k, weight in enumerate((d_gate, d_up)):
        part = dot_nt(feeds, weight[...].reshape(hidden_here, quarter)).astype(jnp.bfloat16)
        pre_out[:, :, k * hidden_here : (k + 1) * hidden_here] = part.reshape(
            nx, all_toks // nx, hidden_here
        )
    pre_copies = [
        send(pre_out.at[lax.rem(x + r, nx)], pre_in.at[r - 1], x_dev(r)) for r in range(1, nx)
    ]

    from_left, from_right, from_far = [], [], []
    for q in range(np_):
        if q:
            row_copies[q].wait_recv()
        from_left.append(send(rows_in.at[q], rows_x.at[0, q], x_dev(1)))
        from_right.append(send(rows_in.at[q], rows_x.at[1, q], x_dev(nx - 1)))

    arrive(pre_copies)
    pre = pre_out[x].astype(jnp.float32)
    for r in range(1, nx):
        pre += pre_in[r - 1].astype(jnp.float32)
    hidden_x[x] = (jax.nn.silu(pre[:, :hidden_here]) * pre[:, hidden_here:]).astype(jnp.bfloat16)
    hidden_copies = [send(hidden_x.at[x], hidden_x.at[x], x_dev(r)) for r in range(1, nx)]

    for q in range(half):
        from_left[q].wait_recv()
        from_far.append(send(rows_x.at[0, q], rows_x.at[2, q], x_dev(1)))
        from_right[half + q].wait_recv()
        from_far.append(send(rows_x.at[1, half + q], rows_x.at[2, half + q], x_dev(nx - 1)))
    for copy in own_expert:
        copy.wait()

    def of_share(taken, share):
        taken = taken.reshape(rows, quarter)
        return dot(taken, w_gate[share]), dot(taken, w_up[share])

    gate_value, up_value = of_share(rows_in[...], x)
    arrive(from_left[half:])
    more = of_share(rows_x[0], lax.rem(x + nx - 1, nx))
    gate_value, up_value = gate_value + more[0], up_value + more[1]
    arrive(from_right[:half])
    more = of_share(rows_x[1], lax.rem(x + 1, nx))
    gate_value, up_value = gate_value + more[0], up_value + more[1]
    arrive(from_far)
    more = of_share(rows_x[2], lax.rem(x + 2, nx))
    gate_value, up_value = gate_value + more[0], up_value + more[1]
    hidden = (jax.nn.silu(gate_value) * up_value).astype(jnp.bfloat16)

    cut = rows // 2
    low, high = hidden[:cut], hidden[cut:]
    right, left, far = lax.rem(x + 1, nx), lax.rem(x + nx - 1, nx), lax.rem(x + 2, nx)

    def put_out(k, values, device):
        sum_out[k] = values.astype(jnp.bfloat16)
        return send(sum_out.at[k], sum_in.at[k], device)

    to_right, to_left = x_dev(1), x_dev(nx - 1)
    sums = [
        put_out(0, dot(low, w_down[far]), to_right),
        put_out(1, dot(high, w_down[far]), to_left),
        put_out(2, dot(high, w_down[right]), to_right),
        put_out(3, dot(low, w_down[left]), to_left),
    ]
    value = dot(low, w_down[right])
    sums[0].wait_recv()
    sums.append(put_out(4, value + sum_in[0].astype(jnp.float32), to_right))
    value = dot(high, w_down[left])
    sums[1].wait_recv()
    sums.append(put_out(5, value + sum_in[1].astype(jnp.float32), to_left))

    arrive(hidden_copies)
    down = d_down[...].reshape(hidden_here, quarter)
    dense_part = dot(hidden_x[...].reshape(all_toks, hidden_here), down)
    arrive(pick_copies)
    table = pick_z[...].reshape(all_toks, LANES)
    dense_part = dense_part * table[:, experts : experts + 1]
    table_hi = table.astype(jnp.bfloat16)
    table_lo = (table - table_hi.astype(jnp.float32)).astype(jnp.bfloat16)
    j_col = iota((all_toks, rows), 1)
    take = (dot(codes, choose) == slot_of(j_col)) & (
        block_of(j_col) == iota((all_toks, rows), 0) >> shift_of(toks)
    )
    take_hi = jnp.where(take, dot(table_hi, choose), 0.0).astype(jnp.bfloat16)
    take_lo = jnp.where(take, dot(table_lo, choose), 0.0).astype(jnp.bfloat16)

    done_low = dot(low, w_down[x])
    done_high = dot(high, w_down[x])
    sums[3].wait_recv()
    sums[4].wait_recv()
    done_low += sum_in[3].astype(jnp.float32) + sum_in[4].astype(jnp.float32)
    back_out[:half] = done_low.astype(jnp.bfloat16).reshape(half, nz * cap, quarter)
    back_in[0] = back_out[0]
    back = [None] + [
        send(back_out.at[q], back_in.at[q], p_dev(np_ - q)) for q in range(1, half)
    ]
    sums[2].wait_recv()
    sums[5].wait_recv()
    done_high += sum_in[2].astype(jnp.float32) + sum_in[5].astype(jnp.float32)
    back_out[half:] = done_high.astype(jnp.bfloat16).reshape(half, nz * cap, quarter)
    back += [send(back_out.at[q], back_in.at[q], p_dev(np_ - q)) for q in range(half, np_)]

    arrive(back[1:])
    results = back_in[...].reshape(rows, quarter)
    part = dot(take_hi, results) + dot(take_lo, results) + dense_part
    last_out[...] = part.astype(jnp.bfloat16).reshape(nz, toks, quarter)
    last = [send(last_out.at[r], last_in.at[r - 1], z_dev(nz - r)) for r in range(1, nz)]
    combined = part[:toks]
    gain = in_row(out_gain)
    arrive(stream_copies)
    stream_part = stream_in[...].astype(jnp.float32).reshape(toks, quarter)
    arrive(last)
    for r in range(1, nz):
        combined += last_in[r - 1].astype(jnp.float32)

    square = jnp.sum(combined * combined, axis=1, keepdims=True)
    on_lane = iota((toks, LANES), 0) == iota((toks, LANES), 1)
    as_row = jnp.sum(jnp.where(on_lane, square, 0.0), axis=0, keepdims=True)
    square_x[0] = jnp.broadcast_to(as_row, square_x.shape[1:])
    square_copies = [send(square_x.at[0], square_x.at[r], x_dev(r)) for r in range(1, nx)]
    combined = combined * gain
    arrive(square_copies)
    all_rows = square_x[0]
    for r in range(1, nx):
        all_rows += square_x[r]
    total_square = jnp.sum(jnp.where(on_lane, all_rows[0:1], 0.0), axis=1, keepdims=True)
    scale = lax.rsqrt(total_square / width + norm_eps)
    layer_out[...] = (stream_part + combined * scale).astype(jnp.bfloat16)

    for copy in started:
        copy.wait_send()


def copies_of(nz, np_, nx):
    x_copies = 3 * (nx - 1) + 3 * (nx - 1) + (nx - 1) + 2 * np_ + np_ + 6
    return x_copies + 4 * (nz - 1) + 5 * (np_ - 1)


def after_mixer(sizes, gated, resid, params):
    nz, ny, nc, nx, cap = sizes
    np_ = ny * nc
    toks, width = resid.shape
    own, quarter = toks // nx, width // nx
    rows = np_ * nz * cap
    all_toks = nz * toks
    bf16, f32 = jnp.bfloat16, jnp.float32
    share = params["expert_gate"].shape[2]
    hid = params["dense_gate"].shape[0]
    tall = lambda a: a.reshape(-1, LANES)
    operands = (
        gated,
        params["proj_out"],
        resid.reshape(nx, own, width),
        tall(params["post_gain"]),
        tall(params["ffn_gain"]),
        tall(params["dense_switch"]),
        params["group_router"].T,
        params["expert_router"].T,
        params["route_experts"].T,
        params["expert_gate"].reshape(nx, quarter, share),
        params["expert_up"].reshape(nx, quarter, share),
        params["expert_down"].reshape(share, width),
        params["dense_gate"],
        params["dense_up"],
        params["dense_down"],
        tall(params["out_gain"]),
    )
    vmem = pl.BlockSpec(memory_space=pltpu.VMEM)
    anyw = pl.BlockSpec(memory_space=pl.ANY)
    in_specs = [vmem] * 9 + [anyw] * 6 + [vmem]
    scratch = [
        pltpu.VMEM((nx, quarter, share), bf16),
        pltpu.VMEM((nx, quarter, share), bf16),
        pltpu.VMEM((nx, share, quarter), bf16),
        pltpu.VMEM((np_, hid, quarter), bf16),
        pltpu.VMEM((np_, hid, quarter), bf16),
        pltpu.VMEM((np_, hid, quarter), bf16),
        pltpu.VMEM((nx, own, width), f32),
        pltpu.VMEM((nx, own, width), bf16),
        pltpu.VMEM((nx - 1, own, width), bf16),
        pltpu.VMEM((nx, own, quarter), bf16),
        pltpu.VMEM((nx, own, quarter), bf16),
        pltpu.VMEM((nx, own, quarter), bf16),
        pltpu.VMEM((nx, own, quarter), bf16),
        pltpu.VMEM((nx, own, LANES), f32),
        pltpu.VMEM((nz, toks, LANES), f32),
        pltpu.VMEM((nz, toks, LANES), bf16),
        pltpu.VMEM((nz, toks, quarter), bf16),
        pltpu.VMEM((np_, nz * cap, quarter), bf16),
        pltpu.VMEM((np_, nz * cap, quarter), bf16),
        pltpu.VMEM((3, np_, nz * cap, quarter), bf16),
        pltpu.VMEM((nx, all_toks // nx, 2 * np_ * hid), bf16),
        pltpu.VMEM((nx - 1, all_toks // nx, 2 * np_ * hid), bf16),
        pltpu.VMEM((nx, all_toks // nx, np_ * hid), bf16),
        pltpu.VMEM((6, rows // 2, quarter), bf16),
        pltpu.VMEM((6, rows // 2, quarter), bf16),
        pltpu.VMEM((np_, nz * cap, quarter), bf16),
        pltpu.VMEM((np_, nz * cap, quarter), bf16),
        pltpu.VMEM((nz, toks, quarter), bf16),
        pltpu.VMEM((nz - 1, toks, quarter), bf16),
        pltpu.VMEM((nx, 8, LANES), f32),
        pltpu.SemaphoreType.DMA((copies_of(nz, np_, nx),)),
        pltpu.SemaphoreType.DMA((copies_of(nz, np_, nx),)),
        pltpu.SemaphoreType.DMA((5 + nx,)),
    ]
    return pl.pallas_call(
        functools.partial(rest_of_layer, sizes),
        out_shape=jax.ShapeDtypeStruct((toks, quarter), bf16),
        in_specs=in_specs,
        out_specs=vmem,
        scratch_shapes=scratch,
        compiler_params=pltpu.CompilerParams(
            collective_id=0, has_side_effects=True, vmem_limit_bytes=56 * 1024 * 1024
        ),
        name="rest_of_layer",
    )(*operands)


def scaled_rows(values, gain):
    values = values.astype(jnp.float32)
    mean_square = jnp.mean(values * values, axis=-1, keepdims=True)
    return values * lax.rsqrt(mean_square + norm_eps) * gain.astype(jnp.float32)


def mixer(p):
    tp_index = lax.axis_index("tp")
    resid, scan_state, conv_state = p["resid"], p["scan_state"], p["conv_state"]
    seqs = resid.shape[0]
    heads_here, head_dim, state_dim = scan_state.shape[1:]
    channels = conv_state.shape[3]
    repeat = heads_here // (channels // state_dim)
    normed = scaled_rows(resid, p["mix_gain"]).astype(jnp.bfloat16)
    fresh = jnp.stack([dot(normed, p["proj_x"]), dot(normed, p["proj_b"]), dot(normed, p["proj_c"])], axis=1).astype(jnp.bfloat16)
    gate_z = dot(normed, p["proj_z"])
    step_all = dot(normed, p["proj_step"])
    step_raw = lax.dynamic_slice_in_dim(step_all, tp_index * heads_here, heads_here, 1)
    history = jnp.concatenate([conv_state, fresh[:, :, None, :]], axis=2)
    activated = jax.nn.silu(
        jnp.sum(history.astype(jnp.float32) * p["conv_taps"].astype(jnp.float32)[None], axis=2)
    )
    xs_heads = activated[:, 0].reshape(seqs, heads_here, head_dim)
    b_heads = jnp.repeat(activated[:, 1].reshape(seqs, -1, state_dim), repeat, axis=1)
    c_heads = jnp.repeat(activated[:, 2].reshape(seqs, -1, state_dim), repeat, axis=1)
    step = jax.nn.softplus(step_raw + p["step_bias"])
    keep = jnp.exp(-p["decay_rate"] * step)
    driven = step[:, :, None] * xs_heads
    new_state = keep[:, :, None, None] * scan_state + driven[:, :, :, None] * b_heads[:, :, None, :]
    read = jnp.sum(new_state * c_heads[:, :, None, :], axis=3).reshape(seqs, channels)
    gated = (read * jax.nn.silu(gate_z) * p["inner_gain"].astype(jnp.float32)).astype(jnp.bfloat16)
    return gated, new_state, history[:, :, 1:, :]


NAMES = (
    "resid",
    "mix_gain",
    "proj_x",
    "proj_z",
    "proj_b",
    "proj_c",
    "proj_step",
    "step_bias",
    "decay_rate",
    "conv_taps",
    "conv_state",
    "scan_state",
    "inner_gain",
    "proj_out",
    "post_gain",
    "ffn_gain",
    "group_router",
    "expert_router",
    "route_experts",
    "expert_gate",
    "expert_up",
    "expert_down",
    "dense_switch",
    "dense_gate",
    "dense_up",
    "dense_down",
    "out_gain",
)


def on_device(*arrays):
    params = dict(zip(NAMES, arrays))
    sizes = tuple(lax.axis_size(a) for a in EP) + (lax.axis_size("tp"), CAPACITY)
    gated, new_state, new_conv = mixer(params)
    layer_out = after_mixer(sizes, gated, params["resid"], params)
    return layer_out, new_state, new_conv


TORUS = (8, 4, 2)


def solution(mesh):
    torus = Mesh(mesh.devices.reshape(*TORUS, mesh.shape["tp"]), EP + ("tp",))
    in_specs = (
        P(EP, None),
        P(),
        P(None, "tp"),
        P(None, "tp"),
        P(None, "tp"),
        P(None, "tp"),
        P(),
        P("tp"),
        P("tp"),
        P(None, None, "tp"),
        P(EP, None, None, "tp"),
        P(EP, "tp", None, None),
        P("tp"),
        P("tp", None),
        P(),
        P(),
        P(),
        P(),
        P(EP, None),
        P(EP, None, "tp"),
        P(EP, None, "tp"),
        P(EP, "tp", None),
        P(),
        P(EP, "tp"),
        P(EP, "tp"),
        P(EP, "tp"),
        P("tp"),
    )
    out_specs = (P(EP, "tp"), P(EP, "tp", None, None), P(EP, None, None, "tp"))
    return jax.shard_map(
        on_device, mesh=torus, in_specs=in_specs, out_specs=out_specs, check_vma=False
    )
```

time: 197 us -> 87.2 us (0.44)
  Pallas kernels: 0 us -> 70.9 us
  blocking collectives: 59.3 us -> 0 us
  waiting for transfers between devices: 56.2 us -> 0 us
  starting transfers between devices: 24.3 us -> 0 us
  between operations: 14.3 us -> 0.75 us
  local copies, waits for them, and re-layouts: 14.4 us -> 2.39 us
  matrix products: 14.4 us -> 5.93 us
  other arithmetic: 12 us -> 6.91 us
    pallas_call x0 -> x1, Pallas kernels: none -> 70.9 us  [after_mixer(): pl.pallas_call(functools.partial(rest_of_layer, sizes), out_shape=jax.Sha...]
    all_to_all x3 -> x0, blocking collectives: 45.8 us -> none  [the longest x1 23.7 us: on_device(): lax.all_to_all(outgoing, EP, split_axis=0, concat_axis=0, tiled=True)]
    all_to_all x6 -> x0, waiting for transfers between devices: 37.1 us -> none  [the longest x4 23.4 us: sent_to_all(): lax.all_to_all(jnp.broadcast_to(array[None], (count, *array.shape)), axis...]
    all_to_all x6 -> x0, starting transfers between devices: 24.2 us -> none  [the longest x4 15.5 us: sent_to_all(): lax.all_to_all(jnp.broadcast_to(array[None], (count, *array.shape)), axis...]
    all_gather x3 -> x0, waiting for transfers between devices: 18.5 us -> none  [the longest x1 18.5 us: sent_together(): result = lax.all_gather(both, axis, axis=dim, tiled=True)]
    all_gather x1 -> x0, blocking collectives: 13.5 us -> none  [all_blocks(): pieces = lax.all_gather(pieces, axes[k], axis=0, tiled=True)]
    dot_general x14 -> x5, matrix products: 14.4 us -> 5.93 us  [dot(): return jnp.dot(a, b, preferred_element_type=jnp.float32)]
    broadcast_in_dim x6 -> x0, local copies, waits for them, and re-layouts: 3.53 us -> none  [the longest x5 3.5 us: sent_to_all(): jnp.broadcast_to(array[None], (count, *array.shape))]
  transfers between devices with their start and end apart: 9 -> 0, of which waited for: 6 -> 0; matrix products, arithmetic and copies ran while one was open for 18% -> 0% of each run, Pallas kernels for 0% -> 0%
where the time goes in v1:
time: 87.2 us; the launch traced here: 86.9 us
  Pallas kernels  70.9 us (81%)
  other arithmetic  6.91 us (8%)
  matrix products  5.93 us (7%)
  local copies, waits for them, and re-layouts  2.39 us (3%)
    pallas_call x1, Pallas kernels, after_mixer(): pl.pallas_call(functools.partial(rest_of_layer, sizes), out_shape=jax.Sha...  70.9 us
    dot_general x5, matrix products, dot(): return jnp.dot(a, b, preferred_element_type=jnp.float32)  5.93 us
    reduce_sum x1, other arithmetic, mixer(): jnp.sum(new_state * c_heads[:, :, None, :], axis=3).reshape(seqs, channels)  2.1 us

profile of v1, /device:TPU:8, one launch (start us, length us, event | category | flops | bytes accessed | tf_op | source)
XLA Modules:
  0.0 86.9 jit_solution(18106723479451904275)
XLA Ops:
  0.6 0.0 copy-start
  0.6 0.0 copy-start.2
  0.7 0.0 copy-start.4
  0.7 0.8 neg.15
  1.5 0.7 convert_element_type.34
  2.2 1.0 %fusion.3 = f32[32]{0:T(128)S(1)} fusion(bf16[32,2048]{1,0:T(8,128)(2,1)} %param.27), kind=kLoop, calls=%fused_computation.10 | loop fusion | flops 196576 | bytes 131200 | tf_op jit(solution)/shard_map/reduce_sum | solution.py:511
  3.2 0.7 convert_element_type.33
  3.9 0.7 convert_element_type.30
  4.6 1.1 %fusion.11 = f32[32,8]{0,1:T(8,128)S(1)} fusion(bf16[2048,8]{0,1:T(8,128)(2,1)} %param.33, bf16[32,2048]{1,0:T(8,128)(2,1)} %param.27, f32[2048]{0:T(1024)S(1)} %convert_element_type.30, f32[32]{0:T(128)S(1)} %add_rsqrt_fusion), kind=kOutput, calls=%fused_computation.24 | convolution fusion | flops 1310720 | bytes 173184 | tf_op jit(solution)/shard_map/dot_general | solution.py:19
  5.7 0.7 multiply_exponential_fusion
  6.5 0.0 copy-done
  6.5 1.2 %fusion = bf16[32,1,1,128]{3,0,2,1:T(8,128)(2,1)S(1)} fusion(bf16[2048,128]{1,0:T(8,128)(2,1)S(1)} %copy-done, bf16[32,2048]{1,0:T(8,128)(2,1)} %param.27, f32[2048]{0:T(1024)S(1)} %convert_element_type.30, f32[32]{0:T(128)S(1)} %add_rsqrt_fusion), kind=kOutput, calls=%fused_computation.5 | convolution fusion | flops 17043456 | bytes 671872 | tf_op jit(solution)/shard_map/dot_general | solution.py:19
  7.6 1.4 %fusion.1 = bf16[32,1,1,128]{3,0,2,1:T(8,128)(2,1)S(1)} fusion(bf16[2048,128]{1,0:T(8,128)(2,1)} %param.31, bf16[32,2048]{1,0:T(8,128)(2,1)} %param.27, f32[2048]{0:T(1024)S(1)} %convert_element_type.30, f32[32]{0:T(128)S(1)} %add_rsqrt_fusion), kind=kOutput, calls=%fused_computation.6 | convolution fusion | flops 17043456 | bytes 671872 | tf_op jit(solution)/shard_map/dot_general | solution.py:19
  9.0 1.4 %fusion.2 = bf16[32,1,1,128]{3,0,2,1:T(8,128)(2,1)S(1)} fusion(bf16[2048,128]{1,0:T(8,128)(2,1)} %param.32, bf16[32,2048]{1,0:T(8,128)(2,1)} %param.27, f32[2048]{0:T(1024)S(1)} %convert_element_type.30, f32[32]{0:T(128)S(1)} %add_rsqrt_fusion), kind=kOutput, calls=%fused_computation.7 | convolution fusion | flops 17043456 | bytes 671872 | tf_op jit(solution)/shard_map/dot_general | solution.py:19
  10.4 0.1 copy.30
  10.5 0.1 copy.31
  10.6 0.0 copy-done.4
  10.7 0.1 reshape_squeeze.3
  10.8 0.1 broadcast_multiply_fusion
  10.9 0.6 slice.25
  11.5 0.0 copy-done.2
  11.5 0.0 copy-start.1
  11.5 0.0 copy-start.3
  11.5 2.1 %multiply_reduce_fusion = (f32[32,2,64]{2,1,0:T(2,128)S(1)}, f32[32,2,64,128]{3,2,1,0:T(8,128)}) fusion(f32[32,128]{1,0:T(8,128)S(1)} %get-tuple-element.10, f32[32,128]{1,0:T(8,128)S(1)} %get-tuple-element.11, f32[32,2,64]{2,1,0:T(2,128)S(1)} %broadcast_multiply_fusion, f32[32,2,64,128]{3,2,1,0:T(8,128)S(1)} %copy-done.2, f32[32,2]{1,0:T(8,128)S(1)} %copy.30), kind=kLoop, calls=%fused_computation | loop fusion | flops 2617344 | bytes 4260096 | tf_op jit(solution)/shard_map/reduce_sum | solution.py:538
  13.6 0.1 reshape.103
  13.7 0.0 copy-done.1
  13.7 0.0 copy-done.3
  13.7 0.9 %multiply_convert_fusion.gated = bf16[32,128]{1,0:T(8,128)(2,1)} fusion(f32[32,128]{1,0:T(8,128)S(1)} %reshape.103, f32[128]{0:T(128)S(1)} %convert_element_type.34, bf16[2048,128]{1,0:T(8,128)(2,1)S(1)} %copy-done.3, bf16[32,2048]{1,0:T(8,128)(2,1)S(1)} %copy-done.1, f32[2048]{0:T(1024)S(1)} %convert_element_type.30, f32[32]{0:T(128)S(1)} %add_rsqrt_fusion), kind=kOutput, calls=%fused_computation.18 | convolution fusion | flops 17068032 | bytes 688768 | tf_op jit(solution)/shard_map/dot_general | solution.py:19
  14.6 70.9 %rest_of_layer.1 = bf16[32,512]{1,0:T(8,128)(2,1)} custom-call(bf16[32,128]{1,0:T(8,128)(2,1)} %multiply_convert_fusion.gated, bf16[128,2048]{1,0:T(8,128)(2,1)} %proj_out.1, bf16[4,8,2048]{2,1,0:T(8,128)(2,1)} %bitcast.28, bf16[16,128]{1,0:T(8,128)(2,1)} %bitcast.34, bf16[16,128]{1,0:T(8,128)(2,1)} %bitcast.35, bf16[16,128]{1,0:T(8,128)(2,1)} %bitcast.36, ...), custom_call_target="tpu_custom_call" | custom-call | tf_op jit(solution)/shard_map/rest_of_layer/pallas_call | solution.py:496
  85.5 1.4 %copy.33 = bf16[32,512]{1,0:T(8,128)(2,1)} copy(bf16[32,512]{1,0:T(8,128)(2,1)} %rest_of_layer.1) | data formatting | bytes 65536
  (4 shorter events, 0.1 us)
Async XLA Ops:
  0.6 5.8 %copy-start = (bf16[2048,128]{1,0:T(8,128)(2,1)S(1)}, bf16[2048,128]{1,0:T(8,128)(2,1)}, u32[]{:S(2)}) copy-start(bf16[2048,128]{1,0:T(8,128)(2,1)} %param.29) | copy-start | bytes 1572868
  0.6 10.9 %copy-start.2 = (f32[32,2,64,128]{3,2,1,0:T(8,128)S(1)}, f32[32,2,64,128]{3,2,1,0:T(8,128)}, u32[]{:S(2)}) copy-start(f32[32,2,64,128]{3,2,1,0:T(8,128)} %param.38) | copy-start | bytes 6291460
  0.7 9.9 %copy-start.4 = (bf16[32,3,3,128]{3,0,2,1:T(8,128)(2,1)S(1)}, bf16[32,3,3,128]{3,0,2,1:T(8,128)(2,1)}, u32[]{:S(2)}) copy-start(bf16[32,3,3,128]{3,0,2,1:T(8,128)(2,1)} %param.37) | copy-start | bytes 221188
  11.5 2.2 %copy-start.1 = (bf16[32,2048]{1,0:T(8,128)(2,1)S(1)}, bf16[32,2048]{1,0:T(8,128)(2,1)}, u32[]{:S(2)}) copy-start(bf16[32,2048]{1,0:T(8,128)(2,1)} %param.27) | copy-start | bytes 393220
  11.5 2.2 %copy-start.3 = (bf16[2048,128]{1,0:T(8,128)(2,1)S(1)}, bf16[2048,128]{1,0:T(8,128)(2,1)}, u32[]{:S(2)}) copy-start(bf16[2048,128]{1,0:T(8,128)(2,1)} %param.30) | copy-start | bytes 1572868

commit v2 on v1

v2 whole, which is shorter than its diff:
```python
import functools

import jax
import jax.numpy as jnp
from jax import lax
from jax.experimental import pallas as pl
from jax.experimental.pallas import tpu as pltpu
from jax.sharding import Mesh
from jax.sharding import PartitionSpec as P

EP = ("ep_0", "ep_1", "ep_2")
MESH = pl.DeviceIdType.MESH
norm_eps = 1e-06
CAPACITY = 4
LANES = 128


def dot(a, b):
    return jnp.dot(a, b, preferred_element_type=jnp.float32)


def dot_nt(a, b):
    return lax.dot_general(a, b, (((1,), (1,)), ((), ())), preferred_element_type=jnp.float32)


def in_row(gain_ref):
    gain = gain_ref[...].astype(jnp.float32)
    return jnp.concatenate([gain[i : i + 1] for i in range(gain.shape[0])], axis=1)


def iota(shape, dim):
    return lax.broadcasted_iota(jnp.int32, shape, dim)


def shift_of(count):
    return count.bit_length() - 1


def root_mean(values):
    return values * lax.rsqrt(jnp.mean(values * values, axis=-1, keepdims=True) + norm_eps)


OPERANDS = (
    "resid",
    "mix_gain",
    "proj_x",
    "proj_b",
    "proj_c",
    "proj_z",
    "proj_step",
    "conv_taps",
    "conv_state",
    "step_bias",
    "decay_rate",
    "scan_state",
    "inner_gain",
    "proj_out",
    "route_experts",
    "dense_gate",
    "dense_up",
    "dense_down",
    "post_gain",
    "ffn_gain",
    "expert_router",
    "group_router",
    "dense_switch",
    "out_gain",
    "expert_gate",
    "expert_up",
    "expert_down",
)


def near_first(nz):
    return sorted(range(nz), key=lambda r: (min(r, nz - r), r))


def layer(sizes, plan, *refs):
    nz, ny, nc, nx, cap = sizes
    np_ = ny * nc
    given = dict(zip(OPERANDS, refs))
    layer_out, state_rows, fresh_out = refs[len(OPERANDS) : len(OPERANDS) + 3]
    s = dict(zip(plan, refs[len(OPERANDS) + 3 :]))
    send_sem, recv_sem, local_sem = s["send_sem"], s["recv_sem"], s["local_sem"]
    z, y, c, x = (lax.axis_index(a) for a in ("ep_0", "ep_1", "ep_2", "tp"))
    place = y * nc + c
    own, width = given["resid"].shape[1:]
    toks = own * nx
    quarter = width // nx
    hz = nz // 2
    half_toks = hz * toks
    chunk = hz * cap
    rows = np_ * chunk
    half = np_ // 2
    order = near_first(nz)

    def z_dev(r):
        return {"ep_0": lax.rem(z + r, nz)}

    def p_dev(q):
        to = lax.rem(place + q, np_)
        return {"ep_1": to // nc, "ep_2": lax.rem(to, nc)}

    def x_dev(r):
        return {"tp": lax.rem(x + r, nx)}

    used = [0]
    started = []

    def send(src, dst, device):
        k = used[0]
        used[0] += 1
        copy = pltpu.make_async_remote_copy(
            src_ref=src,
            dst_ref=dst,
            send_sem=send_sem.at[k],
            recv_sem=recv_sem.at[k],
            device_id=device,
            device_id_type=MESH,
        )
        copy.start()
        started.append(copy)
        return copy

    local_used = [0]

    def fetch(src, dst):
        copy = pltpu.make_async_copy(src, dst, local_sem.at[local_used[0]])
        local_used[0] += 1
        copy.start()
        return copy

    def arrive(copies):
        for copy in copies:
            copy.wait_recv()

    barrier = pltpu.get_barrier_semaphore()
    peers = (
        [x_dev(r) for r in range(1, nx)]
        + [p_dev(q) for q in range(1, np_)]
        + [z_dev(r) for r in range(1, nz)]
    )
    for device in peers:
        pl.semaphore_signal(barrier, inc=1, device_id=device, device_id_type=MESH)

    fetched = {}
    for name in OPERANDS:
        src = given[name]
        if name in ("proj_x", "proj_b", "proj_c", "proj_z"):
            k = ("proj_x", "proj_b", "proj_c", "proj_z").index(name)
            wide = src.shape[1]
            fetched[name] = [fetch(src, s["proj"].at[:, pl.ds(k * wide, wide)])]
        elif name in ("dense_gate", "dense_up", "dense_down"):
            fetched[name] = [fetch(src, s[name].at[0])]
        elif name == "expert_down":
            fetched[name] = [
                fetch(src.at[:, pl.ds(j * quarter, quarter)], s[name].at[j]) for j in range(nx)
            ]
        else:
            fetched[name] = [fetch(src, s[name])]

    def held(name):
        for copy in fetched.pop(name, ()):
            copy.wait()
        return s[name]

    route_t = held("route_experts")[...]
    picks = route_t.shape[0]
    expert_ids = iota((LANES, toks), 0)
    named = jnp.zeros((LANES, toks), jnp.float32)
    for k in range(picks):
        named += jnp.where(expert_ids == route_t[k : k + 1, :], 1.0, 0.0)
    named_b = named.astype(jnp.bfloat16)
    before = jnp.where(iota((toks, toks), 0) < iota((toks, toks), 1), 1.0, 0.0).astype(jnp.bfloat16)
    code_t = (named * (dot(named_b, before) + 1.0)).astype(jnp.bfloat16)
    eye = jnp.where(iota((toks, toks), 0) == iota((toks, toks), 1), 1.0, 0.0).astype(jnp.bfloat16)
    code_z = s["code_z"]
    code_z[0] = dot_nt(eye, code_t).astype(jnp.bfloat16)

    resid = held("resid")
    gain = in_row(held("mix_gain"))
    normed = root_mean(resid[...].astype(jnp.float32).reshape(toks, width)) * gain
    normed = normed.astype(jnp.bfloat16)
    for name in ("proj_x", "proj_b", "proj_c", "proj_z"):
        for copy in fetched.pop(name):
            copy.wait()
    projected = dot(normed, s["proj"][...])
    step_all = dot_nt(normed, held("proj_step")[...])
    taps = held("conv_taps")[...].astype(jnp.float32)
    old_conv = held("conv_state")
    channels = taps.shape[2]
    acts = []
    fresh_ref = s["fresh"]
    for k in range(3):
        fresh = projected[:, k * channels : (k + 1) * channels].astype(jnp.bfloat16)
        fresh_ref[k] = fresh
        mixed_in = fresh.astype(jnp.float32) * taps[k, 3:4]
        for i in range(3):
            mixed_in += old_conv[k, i].astype(jnp.float32) * taps[k, i : i + 1]
        acts.append(jax.nn.silu(mixed_in))
    xs, bs, cs = acts
    gate_z = projected[:, 3 * channels :]
    bias, rate = held("step_bias")[...], held("decay_rate")[...]
    heads_here = bias.shape[1]
    head_dim = channels // heads_here
    head_of = iota((toks, channels), 1) >> shift_of(head_dim)
    head_col = iota(step_all.shape, 1)
    step = jnp.zeros((toks, channels), jnp.float32)
    keep = jnp.zeros((toks, channels), jnp.float32)
    for h in range(heads_here):
        raw = jnp.sum(
            jnp.where(head_col == x * heads_here + h, step_all, 0.0), axis=1, keepdims=True
        )
        one = jax.nn.softplus(raw + bias[:, h : h + 1])
        step = jnp.where(head_of == h, one, step)
        keep = jnp.where(head_of == h, jnp.exp(-rate[:, h : h + 1] * one), keep)
    driven = step * xs
    rows_ref = s["rows_ref"]
    rows_ref[0] = keep
    rows_ref[1] = driven
    rows_ref[2] = bs
    small_out = [fetch(rows_ref, state_rows), fetch(fresh_ref, fresh_out)]
    c_ref, old_read = s["c_ref"], s["old_read"]
    c_ref[...] = cs
    diag = iota((channels, channels), 0) == iota((channels, channels), 1)
    old_state = held("scan_state")

    @pl.loop(0, toks // 8)
    def _(i):
        at = pl.multiple_of(i * 8, 8)
        c8 = c_ref[pl.ds(at, 8), :]
        out = []
        for t in range(8):
            sums = jnp.sum(old_state[at + t] * c8[t : t + 1], axis=1, keepdims=True)
            out.append(jnp.sum(jnp.where(diag, sums, 0.0), axis=0, keepdims=True))
        old_read[pl.ds(at, 8), :] = jnp.concatenate(out, axis=0)

    read = keep * old_read[...] + driven * jnp.sum(bs * cs, axis=1, keepdims=True)
    gated = (read * jax.nn.silu(gate_z) * in_row(held("inner_gain"))).astype(jnp.bfloat16)

    mixed_f, mixed_b, mixed_in = s["mixed_f"], s["mixed_b"], s["mixed_in"]
    share = dot(gated, held("proj_out")[...]).reshape(nx, own, width)
    mixed_f[...] = share
    mixed_b[...] = share.astype(jnp.bfloat16)

    pl.semaphore_wait(barrier, len(peers))

    copies = [
        send(mixed_b.at[lax.rem(x + r, nx)], mixed_in.at[r - 1], x_dev(r)) for r in range(1, nx)
    ]
    code_copies = [send(code_z.at[0], code_z.at[k], z_dev(order[k])) for k in range(1, nz)]
    dense_copies = []
    for name in ("dense_gate", "dense_up", "dense_down"):
        dense_copies += [send(given[name], s[name].at[q], p_dev(q)) for q in range(1, np_)]

    post_gain, ffn_gain = in_row(held("post_gain")), in_row(held("ffn_gain"))
    resid_own = resid[x].astype(jnp.float32)
    arrive(copies)
    mixed = mixed_f[x]
    for r in range(1, nx):
        mixed += mixed_in[r - 1].astype(jnp.float32)
    stream = (resid_own + root_mean(mixed) * post_gain).astype(jnp.bfloat16)
    feed = (root_mean(stream.astype(jnp.float32)) * ffn_gain).astype(jnp.bfloat16)
    feed_out, feed_in = s["feed_out"], s["feed_in"]
    stream_out, stream_in = s["stream_out"], s["stream_in"]
    for j in range(nx):
        feed_out[j] = feed[:, j * quarter : (j + 1) * quarter]
    feed_in[x] = feed_out[x]
    feed_copies = [
        send(feed_out.at[lax.rem(x + r, nx)], feed_in.at[x], x_dev(r)) for r in range(1, nx)
    ]
    for j in range(nx):
        stream_out[j] = stream[:, j * quarter : (j + 1) * quarter]

    feed_f = feed.astype(jnp.float32)
    expert_rows, group_rows = held("expert_router"), held("group_router")
    experts = expert_rows.shape[0]
    groups = group_rows.shape[0]
    group_size = experts // groups
    token_pick = jnp.where(iota((own, toks), 1) == iota((own, toks), 0) + x * own, 1.0, 0.0)
    own_route = dot_nt(token_pick.astype(jnp.bfloat16), route_t.astype(jnp.bfloat16))
    logits = dot_nt(feed, expert_rows[...])
    lanes = iota((own, experts), 1).astype(jnp.float32)
    weights = []
    for k in range(picks):
        chosen = jnp.sum(
            jnp.where(lanes == own_route[:, k : k + 1], logits, 0.0), axis=1, keepdims=True
        )
        weights.append(jnp.exp(chosen))
    total = functools.reduce(jnp.add, weights)
    group_f = group_rows[...].astype(jnp.float32)
    group_exp = [
        jnp.exp(jnp.sum(feed_f * group_f[g : g + 1], axis=1, keepdims=True)) for g in range(groups)
    ]
    group_total = functools.reduce(jnp.add, group_exp)
    first = own_route[:, 0:1]
    group_weight = jnp.zeros((own, 1), jnp.float32)
    for g in range(groups):
        here = (first >= g * group_size) & (first < (g + 1) * group_size)
        group_weight += jnp.where(here, group_exp[g] / group_total, 0.0)
    switch_row = in_row(held("dense_switch"))
    switch = jax.nn.sigmoid(jnp.sum(feed_f * switch_row, axis=1, keepdims=True))
    all_lanes = iota((own, LANES), 1).astype(jnp.float32)
    pick_table = jnp.where(all_lanes < experts, 0.0, switch)
    for k in range(picks):
        pick_table += jnp.where(
            all_lanes == own_route[:, k : k + 1], weights[k] / total * group_weight, 0.0
        )
    pick_in, pick_z = s["pick_in"], s["pick_z"]
    pick_in[x] = pick_table

    arrive(feed_copies)
    feed_z = s["feed_z"]
    feed_z[0] = feed_in[...].astype(jnp.float32).reshape(toks, quarter).astype(jnp.bfloat16)
    feed_copies = [None] + [
        send(feed_z.at[0], feed_z.at[k], z_dev(order[k])) for k in range(1, nz)
    ]
    pick_copies = [send(pick_in.at[x], pick_in.at[x], x_dev(r)) for r in range(1, nx)]
    stream_in[x] = stream_out[x]
    stream_copies = [
        send(stream_out.at[lax.rem(x + r, nx)], stream_in.at[x], x_dev(r)) for r in range(1, nx)
    ]

    def expert_of(j):
        return z * np_ + ((place + (j >> shift_of(chunk))) & (np_ - 1))

    def block_of(j):
        return (j & (chunk - 1)) >> shift_of(cap)

    def slot_of(j):
        return ((j & (cap - 1)) + 1).astype(jnp.float32)

    arrive(code_copies)
    codes = [
        code_z[h * hz : (h + 1) * hz].reshape(half_toks, LANES) for h in range(2)
    ]
    choose_t = jnp.where(
        iota((rows, LANES), 1) == expert_of(iota((rows, LANES), 0)), 1.0, 0.0
    ).astype(jnp.bfloat16)
    choose = jnp.where(
        iota((LANES, rows), 0) == expert_of(iota((LANES, rows), 1)), 1.0, 0.0
    ).astype(jnp.bfloat16)
    j_row = iota((rows, half_toks), 0)
    same_block = block_of(j_row) == iota((rows, half_toks), 1) >> shift_of(toks)
    put = [
        jnp.where((dot_nt(choose_t, k) == slot_of(j_row)) & same_block, 1.0, 0.0).astype(
            jnp.bfloat16
        )
        for k in codes
    ]

    arrive(pick_copies)
    pick_z[0] = pick_in[...].reshape(toks, LANES)
    pick_copies = [send(pick_z.at[0], pick_z.at[k], z_dev(order[k])) for k in range(1, nz)]

    rows_out, rows_in, rows_x = s["rows_out"], s["rows_in"], s["rows_x"]
    pre_out, pre_in, hidden_x = s["pre_out"], s["pre_in"], s["hidden_x"]
    hidden_here = s["dense_gate"].shape[0] * s["dense_gate"].shape[1]
    row_copies, pre_copies = [], []
    from_left, from_right, from_far = ([], []), ([], []), ([], [])

    def rows_to_experts(h):
        arrive(feed_copies[max(1, h * hz) : (h + 1) * hz])
        feeds = feed_z[h * hz : (h + 1) * hz].reshape(half_toks, quarter)
        rows_out[h] = dot(put[h], feeds).astype(jnp.bfloat16).reshape(np_, chunk, quarter)
        rows_in[h, 0] = rows_out[h, 0]
        row_copies.append(
            [None] + [send(rows_out.at[h, q], rows_in.at[h, q], p_dev(q)) for q in range(1, np_)]
        )
        return feeds

    def dense_sums(h, feeds):
        for k, name in enumerate(("dense_gate", "dense_up")):
            part = dot_nt(feeds, held(name)[...].reshape(hidden_here, quarter))
            part = part.reshape(hz, nx, own, hidden_here).swapaxes(0, 1)
            part = part.reshape(nx, hz * own, hidden_here).astype(jnp.bfloat16)
            pre_out[h, :, :, k * hidden_here : (k + 1) * hidden_here] = part
        pre_copies.append(
            [
                send(pre_out.at[h, lax.rem(x + r, nx)], pre_in.at[h, r - 1], x_dev(r))
                for r in range(1, nx)
            ]
        )

    def rows_over_x(h):
        for q in range(np_):
            if q:
                row_copies[h][q].wait_recv()
            from_left[h].append(send(rows_in.at[h, q], rows_x.at[h, 0, q], x_dev(1)))
            from_right[h].append(send(rows_in.at[h, q], rows_x.at[h, 1, q], x_dev(nx - 1)))

    def pass_on(h):
        for q in range(half):
            from_left[h][q].wait_recv()
            from_far[h].append(send(rows_x.at[h, 0, q], rows_x.at[h, 2, q], x_dev(1)))
            k = half + q
            from_right[h][k].wait_recv()
            from_far[h].append(send(rows_x.at[h, 1, k], rows_x.at[h, 2, k], x_dev(nx - 1)))

    w_gate, w_up, w_down = s["expert_gate"], s["expert_up"], s["expert_down"]

    def of_share(taken, share):
        taken = taken.reshape(rows, quarter)
        return dot(taken, w_gate[share]), dot(taken, w_up[share])

    right, left, far = lax.rem(x + 1, nx), lax.rem(x + nx - 1, nx), lax.rem(x + 2, nx)

    def expert_hidden(h):
        gate_value, up_value = of_share(rows_in[h], x)
        arrive(from_left[h][half:])
        more = of_share(rows_x[h, 0], left)
        gate_value, up_value = gate_value + more[0], up_value + more[1]
        arrive(from_right[h][:half])
        more = of_share(rows_x[h, 1], right)
        gate_value, up_value = gate_value + more[0], up_value + more[1]
        arrive(from_far[h])
        more = of_share(rows_x[h, 2], far)
        gate_value, up_value = gate_value + more[0], up_value + more[1]
        return (jax.nn.silu(gate_value) * up_value).astype(jnp.bfloat16)

    sum_out, sum_in = s["sum_out"], s["sum_in"]
    to_right, to_left = x_dev(1), x_dev(nx - 1)
    cut = rows // 2

    def put_out(h, k, values, device):
        sum_out[h, k] = values.astype(jnp.bfloat16)
        return send(sum_out.at[h, k], sum_in.at[h, k], device)

    def sums_start(h, hidden):
        low, high = hidden[:cut], hidden[cut:]
        return [
            put_out(h, 0, dot(low, w_down[far]), to_right),
            put_out(h, 1, dot(high, w_down[far]), to_left),
            put_out(h, 2, dot(high, w_down[right]), to_right),
            put_out(h, 3, dot(low, w_down[left]), to_left),
        ]

    def sums_pass_on(h, hidden, sums):
        low, high = hidden[:cut], hidden[cut:]
        value = dot(low, w_down[right])
        sums[0].wait_recv()
        sums.append(put_out(h, 4, value + sum_in[h, 0].astype(jnp.float32), to_right))
        value = dot(high, w_down[left])
        sums[1].wait_recv()
        sums.append(put_out(h, 5, value + sum_in[h, 1].astype(jnp.float32), to_left))

    back_out, back_in = s["back_out"], s["back_in"]

    def sums_end(h, hidden, sums):
        done = dot(hidden, w_down[x])
        back = [None]
        for k, (a, b) in enumerate(((3, 4), (2, 5))):
            sums[a].wait_recv()
            sums[b].wait_recv()
            total = done[k * cut : (k + 1) * cut]
            total += sum_in[h, a].astype(jnp.float32) + sum_in[h, b].astype(jnp.float32)
            back_out[h, k * half : (k + 1) * half] = total.astype(jnp.bfloat16).reshape(
                half, chunk, quarter
            )
            if k == 0:
                back_in[h, 0] = back_out[h, 0]
            back += [
                send(back_out.at[h, q], back_in.at[h, q], p_dev(np_ - q))
                for q in range(max(1, k * half), (k + 1) * half)
            ]
        return back[1:]

    def dense_hidden(h):
        arrive(pre_copies[h])
        pre = pre_out[h, x].astype(jnp.float32)
        for r in range(1, nx):
            pre += pre_in[h, r - 1].astype(jnp.float32)
        value = jax.nn.silu(pre[:, :hidden_here]) * pre[:, hidden_here:]
        hidden_x[h, x] = value.astype(jnp.bfloat16)
        return [send(hidden_x.at[h, x], hidden_x.at[h, x], x_dev(r)) for r in range(1, nx)]

    feeds = rows_to_experts(0)
    arrive(dense_copies)
    dense_sums(0, feeds)
    rows_over_x(0)
    feeds = rows_to_experts(1)
    dense_sums(1, feeds)
    pass_on(0)
    rows_over_x(1)
    hidden_copies = [dense_hidden(0)]
    held("expert_gate")
    held("expert_up")
    held("expert_down")
    hidden0 = expert_hidden(0)
    sums0 = sums_start(0, hidden0)
    pass_on(1)
    sums_pass_on(0, hidden0, sums0)
    hidden_copies.append(dense_hidden(1))
    hidden1 = expert_hidden(1)
    sums1 = sums_start(1, hidden1)
    backs = [sums_end(0, hidden0, sums0)]
    sums_pass_on(1, hidden1, sums1)

    arrive(pick_copies)
    j_col = iota((half_toks, rows), 1)
    same_block = block_of(j_col) == iota((half_toks, rows), 0) >> shift_of(toks)
    take, dense_part = [], []
    down = held("dense_down")[...].reshape(hidden_here, quarter)
    for h in range(2):
        table = pick_z[h * hz : (h + 1) * hz].reshape(half_toks, LANES)
        table_hi = table.astype(jnp.bfloat16)
        table_lo = (table - table_hi.astype(jnp.float32)).astype(jnp.bfloat16)
        here = (dot(codes[h], choose) == slot_of(j_col)) & same_block
        take.append(
            [
                jnp.where(here, dot(k, choose), 0.0).astype(jnp.bfloat16)
                for k in (table_hi, table_lo)
            ]
        )
        arrive(hidden_copies[h])
        value = hidden_x[h].astype(jnp.float32).reshape(nx, hz, own, hidden_here)
        value = value.swapaxes(0, 1).reshape(half_toks, hidden_here).astype(jnp.bfloat16)
        dense_part.append(dot(value, down) * table[:, experts : experts + 1])

    last_out, last_in = s["last_out"], s["last_in"]
    last, parts = [], []

    def give_back(h):
        arrive(backs[h])
        results = back_in[h].reshape(rows, quarter)
        part = dot(take[h][0], results) + dot(take[h][1], results) + dense_part[h]
        last_out[h * hz : (h + 1) * hz] = part.astype(jnp.bfloat16).reshape(hz, toks, quarter)
        last.extend(
            send(last_out.at[k], last_in.at[k - 1], z_dev(nz - order[k]))
            for k in range(max(1, h * hz), (h + 1) * hz)
        )
        return part

    combined = give_back(0)[:toks]
    backs.append(sums_end(1, hidden1, sums1))
    give_back(1)
    gain = in_row(held("out_gain"))
    arrive(stream_copies)
    stream_part = stream_in[...].astype(jnp.float32).reshape(toks, quarter)
    for k in range(1, nz):
        last[k - 1].wait_recv()
        combined += last_in[k - 1].astype(jnp.float32)

    square_x = s["square_x"]
    square = jnp.sum(combined * combined, axis=1, keepdims=True)
    on_lane = iota((toks, LANES), 0) == iota((toks, LANES), 1)
    as_row = jnp.sum(jnp.where(on_lane, square, 0.0), axis=0, keepdims=True)
    square_x[0] = jnp.broadcast_to(as_row, square_x.shape[1:])
    square_copies = [send(square_x.at[0], square_x.at[r], x_dev(r)) for r in range(1, nx)]
    combined = combined * gain
    arrive(square_copies)
    all_rows = square_x[0]
    for r in range(1, nx):
        all_rows += square_x[r]
    total_square = jnp.sum(jnp.where(on_lane, all_rows[0:1], 0.0), axis=1, keepdims=True)
    scale = lax.rsqrt(total_square / width + norm_eps)
    layer_out[...] = (stream_part + combined * scale).astype(jnp.bfloat16)

    for copy in started:
        copy.wait_send()
    for copy in small_out:
        copy.wait()


def copies_of(nz, np_, nx):
    x_copies = 6 * (nx - 1) + 4 * (nx - 1) + 4 * np_ + 2 * np_ + 12
    return x_copies + 4 * (nz - 1) + 7 * (np_ - 1)


def run_layer(sizes, p):
    nz, ny, nc, nx, cap = sizes
    np_ = ny * nc
    toks, width = p["resid"].shape
    own, quarter = toks // nx, width // nx
    hz = nz // 2
    bf16, f32 = jnp.bfloat16, jnp.float32
    share = p["expert_gate"].shape[2]
    hid = p["dense_gate"].shape[0]
    channels = p["conv_state"].shape[3]
    state_dim = p["scan_state"].shape[3]

    def tall(a):
        return a.reshape(-1, LANES)

    given = dict(p)
    for name in ("mix_gain", "post_gain", "ffn_gain", "dense_switch", "inner_gain", "out_gain"):
        given[name] = tall(p[name])
    for name in ("proj_step", "expert_router", "group_router", "route_experts"):
        given[name] = p[name].T
    given["resid"] = p["resid"].reshape(nx, own, width)
    given["conv_state"] = p["conv_state"].transpose(1, 2, 0, 3)
    given["scan_state"] = p["scan_state"].reshape(toks, channels, state_dim)
    for name in ("step_bias", "decay_rate"):
        given[name] = p[name].reshape(1, -1)
    given["expert_gate"] = p["expert_gate"].reshape(nx, quarter, share)
    given["expert_up"] = p["expert_up"].reshape(nx, quarter, share)
    given["expert_down"] = p["expert_down"].reshape(share, width)
    operands = [given[name] for name in OPERANDS]
    scratch = {}
    for name in OPERANDS:
        if name not in ("proj_x", "proj_b", "proj_c", "proj_z"):
            scratch[name] = (given[name].shape, given[name].dtype)
    for name in ("dense_gate", "dense_up", "dense_down"):
        scratch[name] = ((np_, hid, quarter), bf16)
    scratch["expert_down"] = ((nx, share, quarter), bf16)
    scratch["proj"] = ((width, 4 * channels), bf16)
    scratch["fresh"] = ((3, toks, channels), bf16)
    scratch["rows_ref"] = ((3, toks, channels), f32)
    scratch["c_ref"] = ((toks, channels), f32)
    scratch["old_read"] = ((toks, channels), f32)
    scratch["mixed_f"] = ((nx, own, width), f32)
    scratch["mixed_b"] = ((nx, own, width), bf16)
    scratch["mixed_in"] = ((nx - 1, own, width), bf16)
    for name in ("feed_out", "feed_in", "stream_out", "stream_in"):
        scratch[name] = ((nx, own, quarter), bf16)
    scratch["pick_in"] = ((nx, own, LANES), f32)
    scratch["pick_z"] = ((nz, toks, LANES), f32)
    scratch["code_z"] = ((nz, toks, LANES), bf16)
    scratch["feed_z"] = ((nz, toks, quarter), bf16)
    for name in ("rows_out", "rows_in", "back_out", "back_in"):
        scratch[name] = ((2, np_, hz * cap, quarter), bf16)
    scratch["rows_x"] = ((2, 3, np_, hz * cap, quarter), bf16)
    scratch["pre_out"] = ((2, nx, hz * own, 2 * np_ * hid), bf16)
    scratch["pre_in"] = ((2, nx - 1, hz * own, 2 * np_ * hid), bf16)
    scratch["hidden_x"] = ((2, nx, hz * own, np_ * hid), bf16)
    for name in ("sum_out", "sum_in"):
        scratch[name] = ((2, 6, np_ * hz * cap // 2, quarter), bf16)
    scratch["last_out"] = ((nz, toks, quarter), bf16)
    scratch["last_in"] = ((nz - 1, toks, quarter), bf16)
    scratch["square_x"] = ((nx, 8, LANES), f32)
    plan = tuple(scratch) + ("send_sem", "recv_sem", "local_sem")
    shapes = [pltpu.VMEM(*scratch[name]) for name in scratch]
    copies = copies_of(nz, np_, nx)
    shapes += [
        pltpu.SemaphoreType.DMA((copies,)),
        pltpu.SemaphoreType.DMA((copies,)),
        pltpu.SemaphoreType.DMA((len(OPERANDS) + nx + 1,)),
    ]
    anyw = pl.BlockSpec(memory_space=pl.ANY)
    return pl.pallas_call(
        functools.partial(layer, sizes, plan),
        out_shape=(
            jax.ShapeDtypeStruct((toks, quarter), bf16),
            jax.ShapeDtypeStruct((3, toks, channels), f32),
            jax.ShapeDtypeStruct((3, toks, channels), bf16),
        ),
        in_specs=[anyw] * len(operands),
        out_specs=(pl.BlockSpec(memory_space=pltpu.VMEM), anyw, anyw),
        scratch_shapes=shapes,
        compiler_params=pltpu.CompilerParams(
            collective_id=0, has_side_effects=True, vmem_limit_bytes=56 * 1024 * 1024
        ),
        name="layer",
    )(*operands)


def finish_step(rows, fresh, conv, result, state, new_state, new_conv, layer_out):
    @pl.when(pl.program_id(0) == 0)
    def _():
        layer_out[...] = result[...]
        new_conv[:, 0:2] = conv[:, 1:3]
        new_conv[:, 2] = fresh[...]

    keep, driven, bs = rows[0], rows[1], rows[2]
    channels = keep.shape[1]
    diag = iota((channels, channels), 0) == iota((channels, channels), 1)
    for t in range(state.shape[0]):
        at = slice(t, t + 1)
        keep_col = jnp.sum(jnp.where(diag, keep[at], 0.0), axis=1, keepdims=True)
        driven_col = jnp.sum(jnp.where(diag, driven[at], 0.0), axis=1, keepdims=True)
        new_state[t] = keep_col * state[t] + driven_col * bs[at]


def finish(rows, fresh, result, p):
    toks, heads, head_dim, state_dim = p["scan_state"].shape
    channels = heads * head_dim
    conv = p["conv_state"].transpose(1, 2, 0, 3)
    state = p["scan_state"].reshape(toks, channels, state_dim)
    block = 8
    whole = pl.BlockSpec(memory_space=pltpu.VMEM)
    piece = pl.BlockSpec((block, channels, state_dim), lambda i: (i, 0, 0))
    new_state, new_conv, layer_out = pl.pallas_call(
        finish_step,
        grid=(toks // block,),
        out_shape=(
            jax.ShapeDtypeStruct(state.shape, state.dtype),
            jax.ShapeDtypeStruct(conv.shape, conv.dtype),
            jax.ShapeDtypeStruct(result.shape, result.dtype),
        ),
        in_specs=[
            pl.BlockSpec((3, block, channels), lambda i: (0, i, 0)),
            whole,
            whole,
            whole,
            piece,
        ],
        out_specs=(piece, whole, whole),
        name="finish",
    )(rows, fresh, conv, result, state)
    return (
        layer_out,
        new_state.reshape(p["scan_state"].shape),
        new_conv.transpose(2, 0, 1, 3),
    )


NAMES = (
    "resid",
    "mix_gain",
    "proj_x",
    "proj_z",
    "proj_b",
    "proj_c",
    "proj_step",
    "step_bias",
    "decay_rate",
    "conv_taps",
    "conv_state",
    "scan_state",
    "inner_gain",
    "proj_out",
    "post_gain",
    "ffn_gain",
    "group_router",
    "expert_router",
    "route_experts",
    "expert_gate",
    "expert_up",
    "expert_down",
    "dense_switch",
    "dense_gate",
    "dense_up",
    "dense_down",
    "out_gain",
)


def on_device(*arrays):
    params = dict(zip(NAMES, arrays))
    sizes = tuple(lax.axis_size(a) for a in EP) + (lax.axis_size("tp"), CAPACITY)
    result, rows, fresh = run_layer(sizes, params)
    return finish(rows, fresh, result, params)


TORUS = (8, 4, 2)


def solution(mesh):
    torus = Mesh(mesh.devices.reshape(*TORUS, mesh.shape["tp"]), EP + ("tp",))
    in_specs = (
        P(EP, None),
        P(),
        P(None, "tp"),
        P(None, "tp"),
        P(None, "tp"),
        P(None, "tp"),
        P(),
        P("tp"),
        P("tp"),
        P(None, None, "tp"),
        P(EP, None, None, "tp"),
        P(EP, "tp", None, None),
        P("tp"),
        P("tp", None),
        P(),
        P(),
        P(),
        P(),
        P(EP, None),
        P(EP, None, "tp"),
        P(EP, None, "tp"),
        P(EP, "tp", None),
        P(),
        P(EP, "tp"),
        P(EP, "tp"),
        P(EP, "tp"),
        P("tp"),
    )
    out_specs = (P(EP, "tp"), P(EP, "tp", None, None), P(EP, None, None, "tp"))
    return jax.shard_map(
        on_device, mesh=torus, in_specs=in_specs, out_specs=out_specs, check_vma=False
    )
```

time: 87.2 us -> 76.4 us (0.88)
  other arithmetic: 6.91 us -> 0 us
  matrix products: 5.93 us -> 0 us
  Pallas kernels: 70.9 us -> 75.6 us
  local copies, waits for them, and re-layouts: 2.39 us -> 0 us
    dot_general x5 -> x0, matrix products: 5.93 us -> none  [dot(): return jnp.dot(a, b, preferred_element_type=jnp.float32)]
    pallas_call x1 -> x2, Pallas kernels: 70.9 us -> 75.6 us  [the longest x1 71.1 us: run_layer(): pl.pallas_call(functools.partial(layer, sizes, plan), out_shape=(jax.Shap...]
    reduce_sum x3 -> x0, other arithmetic: 3.16 us -> none  [the longest x1 2.1 us: mixer(): jnp.sum(new_state * c_heads[:, :, None, :], axis=3).reshape(seqs, channels)]
    convert_element_type x3 -> x0, other arithmetic: 2.04 us -> none  [the longest x1 0.7 us: mixer(): p['conv_taps'].astype(jnp.float32)[None]]
    unnamed x11 -> x0, local copies, waits for them, and re-layouts: 1.4 us -> none
where the time goes in v2:
time: 76.4 us; the launch traced here: 76.2 us
  Pallas kernels  75.6 us (99%)
    pallas_call x1, Pallas kernels, run_layer(): pl.pallas_call(functools.partial(layer, sizes, plan), out_shape=(jax.Shap...  71.1 us
    pallas_call x1, Pallas kernels, finish(): pl.pallas_call(finish_step, grid=(toks // block,), out_shape=(jax.ShapeDt...  4.48 us

profile of v2, /device:TPU:8, one launch (start us, length us, event | category | flops | bytes accessed | tf_op | source)
XLA Modules:
  0.0 76.2 jit_solution(15806451790453310247)
XLA Ops:
  0.6 71.1 %layer.1 = (bf16[32,512]{1,0:T(8,128)(2,1)}, f32[3,32,128]{2,1,0:T(8,128)}, bf16[3,32,128]{2,1,0:T(8,128)(2,1)}) custom-call(bf16[4,8,2048]{2,1,0:T(8,128)(2,1)} %bitcast.28, bf16[16,128]{1,0:T(8,128)(2,1)} %bitcast.31, bf16[2048,128]{1,0:T(8,128)(2,1)} %refs_2_.1, bf16[2048,128]{1,0:T(8,128)(2,1)} %refs_3_.1, bf16[2048,128]{1,0:T(8,128)(2,1)} %refs_4_.1, ...), custom_call_target="tpu_custom_call" | custom-call | tf_op jit(solution)/shard_map/layer/pallas_call | solution.py:640
  71.7 4.5 %finish.1 = (f32[32,128,128]{2,1,0:T(8,128)}, bf16[3,3,32,128]{3,2,1,0:T(8,128)(2,1)}, bf16[32,512]{1,0:T(8,128)(2,1)}) custom-call(f32[3,32,128]{2,1,0:T(8,128)} %get-tuple-element.9.rows, bf16[3,32,128]{2,1,0:T(8,128)(2,1)} %get-tuple-element.10.fresh, bf16[3,3,32,128]{3,2,1,0:T(8,128)(2,1)} %bitcast.26, bf16[32,512]{1,0:T(8,128)(2,1)} %get-tuple-element.11.result, ...), custom_call_target="tpu_custom_call" | custom-call | tf_op jit(solution)/shard_map/finish/pallas_call | solution.py:682

commit v3 on v2

v3 whole, which is shorter than its diff:
```python
import functools
from types import SimpleNamespace

import jax
import jax.numpy as jnp
from jax import lax
from jax.experimental import pallas as pl
from jax.experimental.pallas import tpu as pltpu
from jax.sharding import Mesh
from jax.sharding import PartitionSpec as P

EP = ("ep_0", "ep_1", "ep_2")
MESH = pl.DeviceIdType.MESH
norm_eps = 1e-06
CAPACITY = 4
LANES = 128


def dot(a, b):
    return jnp.dot(a, b, preferred_element_type=jnp.float32)


def dot_nt(a, b):
    return lax.dot_general(a, b, (((1,), (1,)), ((), ())), preferred_element_type=jnp.float32)


def in_row(gain_ref):
    gain = gain_ref[...].astype(jnp.float32)
    return jnp.concatenate([gain[i : i + 1] for i in range(gain.shape[0])], axis=1)


def iota(shape, dim):
    return lax.broadcasted_iota(jnp.int32, shape, dim)


def shift_of(count):
    return count.bit_length() - 1


def root_mean(values):
    return values * lax.rsqrt(jnp.mean(values * values, axis=-1, keepdims=True) + norm_eps)


def far_first(nz):
    return sorted(range(nz), key=lambda r: (-min(r, nz - r), r))


def layer(sizes, plan, *refs):
    nz, ny, nc, nx, cap = sizes
    np_ = ny * nc
    names, scratch = plan
    given = SimpleNamespace(**dict(zip(names, refs)))
    layer_out, state_rows, state_cols, fresh_out = refs[len(names) :][:4]
    send_sem, recv_sem, local_sem = refs[len(names) + 4 :][:3]
    s = SimpleNamespace(**dict(zip(scratch, refs[len(names) + 7 :])))
    z, y, c, x = (lax.axis_index(a) for a in ("ep_0", "ep_1", "ep_2", "tp"))
    place = y * nc + c
    own, width = given.resid.shape[1:]
    toks = own * nx
    quarter = width // nx
    hz = nz // 2
    half_toks = hz * toks
    chunk = hz * cap
    rows = np_ * chunk
    half = np_ // 2
    order = far_first(nz)
    here = order.index(0)
    others = [k for k in range(nz) if k != here]

    def z_dev(r):
        return {"ep_0": lax.rem(z + r, nz)}

    def p_dev(q):
        to = lax.rem(place + q, np_)
        return {"ep_1": to // nc, "ep_2": lax.rem(to, nc)}

    def x_dev(r):
        return {"tp": lax.rem(x + r, nx)}

    used = [0]
    started = []

    def send(src, dst, device):
        k = used[0]
        used[0] += 1
        copy = pltpu.make_async_remote_copy(
            src_ref=src,
            dst_ref=dst,
            send_sem=send_sem.at[k],
            recv_sem=recv_sem.at[k],
            device_id=device,
            device_id_type=MESH,
        )
        copy.start()
        started.append(copy)
        return copy

    local_used = [0]

    def fetch(src, dst):
        copy = pltpu.make_async_copy(src, dst, local_sem.at[local_used[0]])
        local_used[0] += 1
        copy.start()
        return copy

    def arrive(copies):
        for copy in copies:
            copy.wait_recv()

    barrier = pltpu.get_barrier_semaphore()
    peers = (
        [x_dev(r) for r in range(1, nx)]
        + [p_dev(q) for q in range(1, np_)]
        + [z_dev(r) for r in range(1, nz)]
    )
    for device in peers:
        pl.semaphore_signal(barrier, inc=1, device_id=device, device_id_type=MESH)

    def bring(*pairs):
        coming = [fetch(src, dst) for src, dst in pairs]

        def get():
            while coming:
                coming.pop().wait()
            return pairs[0][1]

        return get

    g, ready = given, SimpleNamespace()
    ready.route_experts = bring((g.route_experts, s.route_experts))
    ready.resid = bring((g.resid, s.resid))
    ready.mix_gain = bring((g.mix_gain, s.mix_gain))
    wide = g.proj_x.shape[1]
    ready.proj = bring(
        *(
            (one, s.proj.at[:, pl.ds(k * wide, wide)])
            for k, one in enumerate((g.proj_x, g.proj_b, g.proj_c, g.proj_z))
        )
    )
    ready.proj_step = bring((g.proj_step, s.proj_step))
    ready.conv_taps = bring((g.conv_taps, s.conv_taps))
    ready.conv_state = bring((g.conv_state, s.conv_state))
    ready.step_bias = bring((g.step_bias, s.step_bias))
    ready.decay_rate = bring((g.decay_rate, s.decay_rate))
    ready.scan_state = bring((g.scan_state, s.scan_state))
    ready.inner_gain = bring((g.inner_gain, s.inner_gain))
    ready.proj_out = bring((g.proj_out, s.proj_out))
    ready.post_gain = bring((g.post_gain, s.post_gain))
    ready.ffn_gain = bring((g.ffn_gain, s.ffn_gain))
    ready.expert_router = bring((g.expert_router, s.expert_router))
    ready.group_router = bring((g.group_router, s.group_router))
    ready.dense_switch = bring((g.dense_switch, s.dense_switch))
    ready.out_gain = bring((g.out_gain, s.out_gain))
    ready.dense_gate = bring((g.dense_gate, s.dense_gate.at[0]))
    ready.dense_up = bring((g.dense_up, s.dense_up.at[0]))
    ready.dense_down = bring((g.dense_down, s.dense_down.at[0]))
    ready.expert_gate = bring((g.expert_gate, s.expert_gate))
    ready.expert_up = bring((g.expert_up, s.expert_up))
    ready.expert_down = bring(
        *((g.expert_down.at[:, pl.ds(j * quarter, quarter)], s.expert_down.at[j]) for j in range(nx))
    )

    route_t = ready.route_experts()[...]
    picks = route_t.shape[0]
    expert_ids = iota((LANES, toks), 0)
    named = jnp.zeros((LANES, toks), jnp.float32)
    for k in range(picks):
        named += jnp.where(expert_ids == route_t[k : k + 1, :], 1.0, 0.0)
    named_b = named.astype(jnp.bfloat16)
    before = jnp.where(iota((toks, toks), 0) < iota((toks, toks), 1), 1.0, 0.0).astype(jnp.bfloat16)
    code_t = (named * (dot(named_b, before) + 1.0)).astype(jnp.bfloat16)
    eye = jnp.where(iota((toks, toks), 0) == iota((toks, toks), 1), 1.0, 0.0).astype(jnp.bfloat16)
    code_z = s.code_z
    code_z[here] = dot_nt(eye, code_t).astype(jnp.bfloat16)

    resid = ready.resid()
    gain = in_row(ready.mix_gain())
    normed = root_mean(resid[...].astype(jnp.float32).reshape(toks, width)) * gain
    normed = normed.astype(jnp.bfloat16)
    ready.proj()
    projected = dot(normed, s.proj[...])
    step_all = dot_nt(normed, ready.proj_step()[...])
    taps = ready.conv_taps()[...].astype(jnp.float32)
    old_conv = ready.conv_state()
    channels = taps.shape[2]
    acts = []
    fresh_ref = s.fresh
    for k in range(3):
        fresh = projected[:, k * channels : (k + 1) * channels].astype(jnp.bfloat16)
        fresh_ref[k] = fresh
        mixed_in = fresh.astype(jnp.float32) * taps[k, 3:4]
        for i in range(3):
            mixed_in += old_conv[k, i].astype(jnp.float32) * taps[k, i : i + 1]
        acts.append(jax.nn.silu(mixed_in))
    xs, bs, cs = acts
    gate_z = projected[:, 3 * channels :]
    bias, rate = ready.step_bias()[...], ready.decay_rate()[...]
    heads_here = bias.shape[1]
    head_dim = channels // heads_here
    head_of = iota((toks, channels), 1) >> shift_of(head_dim)
    head_col = iota(step_all.shape, 1)
    step = jnp.zeros((toks, channels), jnp.float32)
    keep = jnp.zeros((toks, channels), jnp.float32)
    rows_ref = s.rows_ref
    for h in range(heads_here):
        raw = jnp.sum(
            jnp.where(head_col == x * heads_here + h, step_all, 0.0), axis=1, keepdims=True
        )
        one = jax.nn.softplus(raw + bias[:, h : h + 1])
        step = jnp.where(head_of == h, one, step)
        kept = jnp.exp(-rate[:, h : h + 1] * one)
        keep = jnp.where(head_of == h, kept, keep)
        rows_ref[h] = jnp.broadcast_to(kept, (toks, channels))
    driven = step * xs
    rows_ref[heads_here] = bs
    s.cols_ref[...] = jnp.concatenate([driven] * (channels // toks), axis=0).T
    small_out = [
        fetch(rows_ref, state_rows),
        fetch(s.cols_ref, state_cols),
        fetch(fresh_ref, fresh_out),
    ]
    c_ref, old_read = s.c_ref, s.old_read
    c_ref[...] = cs
    diag = iota((channels, channels), 0) == iota((channels, channels), 1)
    old_state = ready.scan_state()

    @pl.loop(0, toks // 8)
    def _(i):
        at = pl.multiple_of(i * 8, 8)
        c8 = c_ref[pl.ds(at, 8), :]
        out = []
        for t in range(8):
            sums = jnp.sum(old_state[at + t] * c8[t : t + 1], axis=1, keepdims=True)
            out.append(jnp.sum(jnp.where(diag, sums, 0.0), axis=0, keepdims=True))
        old_read[pl.ds(at, 8), :] = jnp.concatenate(out, axis=0)

    read = keep * old_read[...] + driven * jnp.sum(bs * cs, axis=1, keepdims=True)
    gated = (read * jax.nn.silu(gate_z) * in_row(ready.inner_gain())).astype(jnp.bfloat16)

    mixed_f, mixed_b, mixed_in = s.mixed_f, s.mixed_b, s.mixed_in
    share = dot(gated, ready.proj_out()[...]).reshape(nx, own, width)
    mixed_f[...] = share
    mixed_b[...] = share.astype(jnp.bfloat16)

    pl.semaphore_wait(barrier, len(peers))

    copies = [
        send(mixed_b.at[lax.rem(x + r, nx)], mixed_in.at[r - 1], x_dev(r)) for r in range(1, nx)
    ]
    code_copies = [send(code_z.at[here], code_z.at[k], z_dev(order[k])) for k in others]
    dense_copies = []
    for one, all_here in (
        (g.dense_gate, s.dense_gate),
        (g.dense_up, s.dense_up),
        (g.dense_down, s.dense_down),
    ):
        dense_copies += [send(one, all_here.at[q], p_dev(q)) for q in range(1, np_)]

    post_gain, ffn_gain = in_row(ready.post_gain()), in_row(ready.ffn_gain())
    resid_own = resid[x].astype(jnp.float32)
    arrive(copies)
    mixed = mixed_f[x]
    for r in range(1, nx):
        mixed += mixed_in[r - 1].astype(jnp.float32)
    stream = (resid_own + root_mean(mixed) * post_gain).astype(jnp.bfloat16)
    feed = (root_mean(stream.astype(jnp.float32)) * ffn_gain).astype(jnp.bfloat16)
    feed_out, feed_in = s.feed_out, s.feed_in
    stream_out, stream_in = s.stream_out, s.stream_in
    for j in range(nx):
        feed_out[j] = feed[:, j * quarter : (j + 1) * quarter]
    feed_in[x] = feed_out[x]
    feed_copies = [
        send(feed_out.at[lax.rem(x + r, nx)], feed_in.at[x], x_dev(r)) for r in range(1, nx)
    ]
    for j in range(nx):
        stream_out[j] = stream[:, j * quarter : (j + 1) * quarter]

    feed_f = feed.astype(jnp.float32)
    expert_rows, group_rows = ready.expert_router(), ready.group_router()
    experts = expert_rows.shape[0]
    groups = group_rows.shape[0]
    group_size = experts // groups
    token_pick = jnp.where(iota((own, toks), 1) == iota((own, toks), 0) + x * own, 1.0, 0.0)
    own_route = dot_nt(token_pick.astype(jnp.bfloat16), route_t.astype(jnp.bfloat16))
    logits = dot_nt(feed, expert_rows[...])
    lanes = iota((own, experts), 1).astype(jnp.float32)
    weights = []
    for k in range(picks):
        chosen = jnp.sum(
            jnp.where(lanes == own_route[:, k : k + 1], logits, 0.0), axis=1, keepdims=True
        )
        weights.append(jnp.exp(chosen))
    total = functools.reduce(jnp.add, weights)
    group_f = group_rows[...].astype(jnp.float32)
    group_exp = [
        jnp.exp(jnp.sum(feed_f * group_f[g : g + 1], axis=1, keepdims=True)) for g in range(groups)
    ]
    group_total = functools.reduce(jnp.add, group_exp)
    first = own_route[:, 0:1]
    group_weight = jnp.zeros((own, 1), jnp.float32)
    for g in range(groups):
        in_group = (first >= g * group_size) & (first < (g + 1) * group_size)
        group_weight += jnp.where(in_group, group_exp[g] / group_total, 0.0)
    switch_row = in_row(ready.dense_switch())
    switch = jax.nn.sigmoid(jnp.sum(feed_f * switch_row, axis=1, keepdims=True))
    all_lanes = iota((own, LANES), 1).astype(jnp.float32)
    pick_table = jnp.where(all_lanes < experts, 0.0, switch)
    for k in range(picks):
        pick_table += jnp.where(
            all_lanes == own_route[:, k : k + 1], weights[k] / total * group_weight, 0.0
        )
    pick_in, pick_z = s.pick_in, s.pick_z
    pick_in[x] = pick_table

    arrive(feed_copies)
    feed_z = s.feed_z
    feed_z[here] = feed_in[...].astype(jnp.float32).reshape(toks, quarter).astype(jnp.bfloat16)
    feed_copies = [send(feed_z.at[here], feed_z.at[k], z_dev(order[k])) for k in others]
    pick_copies = [send(pick_in.at[x], pick_in.at[x], x_dev(r)) for r in range(1, nx)]
    stream_in[x] = stream_out[x]
    stream_copies = [
        send(stream_out.at[lax.rem(x + r, nx)], stream_in.at[x], x_dev(r)) for r in range(1, nx)
    ]

    def expert_of(j):
        return z * np_ + ((place + (j >> shift_of(chunk))) & (np_ - 1))

    def block_of(j):
        return (j & (chunk - 1)) >> shift_of(cap)

    def slot_of(j):
        return ((j & (cap - 1)) + 1).astype(jnp.float32)

    arrive(code_copies)
    codes = [
        code_z[h * hz : (h + 1) * hz].reshape(half_toks, LANES) for h in range(2)
    ]
    choose_t = jnp.where(
        iota((rows, LANES), 1) == expert_of(iota((rows, LANES), 0)), 1.0, 0.0
    ).astype(jnp.bfloat16)
    choose = jnp.where(
        iota((LANES, rows), 0) == expert_of(iota((LANES, rows), 1)), 1.0, 0.0
    ).astype(jnp.bfloat16)
    j_row = iota((rows, half_toks), 0)
    same_block = block_of(j_row) == iota((rows, half_toks), 1) >> shift_of(toks)
    put = [
        jnp.where((dot_nt(choose_t, k) == slot_of(j_row)) & same_block, 1.0, 0.0).astype(
            jnp.bfloat16
        )
        for k in codes
    ]

    arrive(pick_copies)
    pick_z[here] = pick_in[...].reshape(toks, LANES)
    pick_copies = [send(pick_z.at[here], pick_z.at[k], z_dev(order[k])) for k in others]

    rows_out, rows_in, rows_x = s.rows_out, s.rows_in, s.rows_x
    pre_out, pre_in, hidden_x = s.pre_out, s.pre_in, s.hidden_x
    hidden_here = s.dense_gate.shape[0] * s.dense_gate.shape[1]
    row_copies, pre_copies = [], []
    from_left, from_right, from_far = ([], []), ([], []), ([], [])

    def rows_to_experts(h):
        arrive(feed_copies[h * hz : (h + 1) * hz])
        feeds = feed_z[h * hz : (h + 1) * hz].reshape(half_toks, quarter)
        rows_out[h] = dot(put[h], feeds).astype(jnp.bfloat16).reshape(np_, chunk, quarter)
        rows_in[h, 0] = rows_out[h, 0]
        row_copies.append(
            [None] + [send(rows_out.at[h, q], rows_in.at[h, q], p_dev(q)) for q in range(1, np_)]
        )
        return feeds

    def dense_sums(h, feeds):
        ready.dense_gate()
        ready.dense_up()
        for k, weight in enumerate((s.dense_gate, s.dense_up)):
            part = dot_nt(feeds, weight[...].reshape(hidden_here, quarter))
            part = part.reshape(hz, nx, own, hidden_here).swapaxes(0, 1)
            part = part.reshape(nx, hz * own, hidden_here).astype(jnp.bfloat16)
            pre_out[h, :, :, k * hidden_here : (k + 1) * hidden_here] = part
        pre_copies.append(
            [
                send(pre_out.at[h, lax.rem(x + r, nx)], pre_in.at[h, r - 1], x_dev(r))
                for r in range(1, nx)
            ]
        )

    def rows_over_x(h):
        for q in range(np_):
            if q:
                row_copies[h][q].wait_recv()
            from_left[h].append(send(rows_in.at[h, q], rows_x.at[h, 0, q], x_dev(1)))
            from_right[h].append(send(rows_in.at[h, q], rows_x.at[h, 1, q], x_dev(nx - 1)))

    def pass_on(h):
        for q in range(half):
            from_left[h][q].wait_recv()
            from_far[h].append(send(rows_x.at[h, 0, q], rows_x.at[h, 2, q], x_dev(1)))
            k = half + q
            from_right[h][k].wait_recv()
            from_far[h].append(send(rows_x.at[h, 1, k], rows_x.at[h, 2, k], x_dev(nx - 1)))

    w_gate, w_up, w_down = s.expert_gate, s.expert_up, s.expert_down

    def of_share(taken, share):
        taken = taken.reshape(rows, quarter)
        return dot(taken, w_gate[share]), dot(taken, w_up[share])

    right, left, far = lax.rem(x + 1, nx), lax.rem(x + nx - 1, nx), lax.rem(x + 2, nx)

    def expert_hidden(h):
        gate_value, up_value = of_share(rows_in[h], x)
        arrive(from_left[h][half:])
        more = of_share(rows_x[h, 0], left)
        gate_value, up_value = gate_value + more[0], up_value + more[1]
        arrive(from_right[h][:half])
        more = of_share(rows_x[h, 1], right)
        gate_value, up_value = gate_value + more[0], up_value + more[1]
        arrive(from_far[h])
        more = of_share(rows_x[h, 2], far)
        gate_value, up_value = gate_value + more[0], up_value + more[1]
        return (jax.nn.silu(gate_value) * up_value).astype(jnp.bfloat16)

    sum_out, sum_in = s.sum_out, s.sum_in
    to_right, to_left = x_dev(1), x_dev(nx - 1)
    cut = rows // 2

    def put_out(h, k, values, device):
        sum_out[h, k] = values.astype(jnp.bfloat16)
        return send(sum_out.at[h, k], sum_in.at[h, k], device)

    def sums_start(h, hidden):
        low, high = hidden[:cut], hidden[cut:]
        return [
            put_out(h, 0, dot(low, w_down[far]), to_right),
            put_out(h, 1, dot(high, w_down[far]), to_left),
            put_out(h, 2, dot(high, w_down[right]), to_right),
            put_out(h, 3, dot(low, w_down[left]), to_left),
        ]

    def sums_pass_on(h, hidden, sums):
        low, high = hidden[:cut], hidden[cut:]
        value = dot(low, w_down[right])
        sums[0].wait_recv()
        sums.append(put_out(h, 4, value + sum_in[h, 0].astype(jnp.float32), to_right))
        value = dot(high, w_down[left])
        sums[1].wait_recv()
        sums.append(put_out(h, 5, value + sum_in[h, 1].astype(jnp.float32), to_left))

    back_out, back_in = s.back_out, s.back_in

    def sums_end(h, hidden, sums):
        done = dot(hidden, w_down[x])
        back = [None]
        for k, (a, b) in enumerate(((3, 4), (2, 5))):
            sums[a].wait_recv()
            sums[b].wait_recv()
            total = done[k * cut : (k + 1) * cut]
            total += sum_in[h, a].astype(jnp.float32) + sum_in[h, b].astype(jnp.float32)
            back_out[h, k * half : (k + 1) * half] = total.astype(jnp.bfloat16).reshape(
                half, chunk, quarter
            )
            if k == 0:
                back_in[h, 0] = back_out[h, 0]
            back += [
                send(back_out.at[h, q], back_in.at[h, q], p_dev(np_ - q))
                for q in range(max(1, k * half), (k + 1) * half)
            ]
        return back[1:]

    def dense_hidden(h):
        arrive(pre_copies[h])
        pre = pre_out[h, x].astype(jnp.float32)
        for r in range(1, nx):
            pre += pre_in[h, r - 1].astype(jnp.float32)
        value = jax.nn.silu(pre[:, :hidden_here]) * pre[:, hidden_here:]
        hidden_x[h, x] = value.astype(jnp.bfloat16)
        return [send(hidden_x.at[h, x], hidden_x.at[h, x], x_dev(r)) for r in range(1, nx)]

    feeds = rows_to_experts(0)
    arrive(dense_copies)
    dense_sums(0, feeds)
    feeds = rows_to_experts(1)
    dense_sums(1, feeds)
    rows_over_x(0)
    pass_on(0)
    rows_over_x(1)
    hidden_copies = [dense_hidden(0)]
    ready.expert_gate()
    ready.expert_up()
    ready.expert_down()
    hidden0 = expert_hidden(0)
    sums0 = sums_start(0, hidden0)
    pass_on(1)
    sums_pass_on(0, hidden0, sums0)
    hidden_copies.append(dense_hidden(1))
    hidden1 = expert_hidden(1)
    sums1 = sums_start(1, hidden1)
    backs = [sums_end(0, hidden0, sums0)]
    sums_pass_on(1, hidden1, sums1)

    arrive(pick_copies)
    j_col = iota((half_toks, rows), 1)
    same_block = block_of(j_col) == iota((half_toks, rows), 0) >> shift_of(toks)
    take, dense_part = [], []
    ready.dense_down()
    down = s.dense_down[...].reshape(hidden_here, quarter)
    for h in range(2):
        table = pick_z[h * hz : (h + 1) * hz].reshape(half_toks, LANES)
        table_hi = table.astype(jnp.bfloat16)
        table_lo = (table - table_hi.astype(jnp.float32)).astype(jnp.bfloat16)
        taken = (dot(codes[h], choose) == slot_of(j_col)) & same_block
        take.append(
            [
                jnp.where(taken, dot(k, choose), 0.0).astype(jnp.bfloat16)
                for k in (table_hi, table_lo)
            ]
        )
        arrive(hidden_copies[h])
        value = hidden_x[h].astype(jnp.float32).reshape(nx, hz, own, hidden_here)
        value = value.swapaxes(0, 1).reshape(half_toks, hidden_here).astype(jnp.bfloat16)
        dense_part.append(dot(value, down) * table[:, experts : experts + 1])

    last_out, last_in = s.last_out, s.last_in
    last, parts = [], []

    def give_back(h):
        arrive(backs[h])
        results = back_in[h].reshape(rows, quarter)
        part = dot(take[h][0], results) + dot(take[h][1], results) + dense_part[h]
        last_out[h * hz : (h + 1) * hz] = part.astype(jnp.bfloat16).reshape(hz, toks, quarter)
        last.extend(
            send(last_out.at[k], last_in.at[k], z_dev(nz - order[k]))
            for k in others[h * hz : (h + 1) * hz]
        )
        return part

    give_back(0)
    backs.append(sums_end(1, hidden1, sums1))
    combined = give_back(1)[(here - hz) * toks : (here - hz + 1) * toks]
    gain = in_row(ready.out_gain())
    arrive(stream_copies)
    stream_part = stream_in[...].astype(jnp.float32).reshape(toks, quarter)
    for k in others:
        last[k].wait_recv()
        combined += last_in[k].astype(jnp.float32)

    square_x = s.square_x
    square = jnp.sum(combined * combined, axis=1, keepdims=True)
    on_lane = iota((toks, LANES), 0) == iota((toks, LANES), 1)
    as_row = jnp.sum(jnp.where(on_lane, square, 0.0), axis=0, keepdims=True)
    square_x[0] = jnp.broadcast_to(as_row, square_x.shape[1:])
    square_copies = [send(square_x.at[0], square_x.at[r], x_dev(r)) for r in range(1, nx)]
    combined = combined * gain
    arrive(square_copies)
    all_rows = square_x[0]
    for r in range(1, nx):
        all_rows += square_x[r]
    total_square = jnp.sum(jnp.where(on_lane, all_rows[0:1], 0.0), axis=1, keepdims=True)
    scale = lax.rsqrt(total_square / width + norm_eps)
    layer_out[...] = (stream_part + combined * scale).astype(jnp.bfloat16)

    for copy in started:
        copy.wait_send()
    for copy in small_out:
        copy.wait()


def copies_of(nz, np_, nx):
    x_copies = 6 * (nx - 1) + 4 * (nx - 1) + 4 * np_ + 2 * np_ + 12
    return x_copies + 4 * (nz - 1) + 7 * (np_ - 1)


def run_layer(sizes, p):
    nz, ny, nc, nx, cap = sizes
    np_ = ny * nc
    toks, width = p.resid.shape
    own, quarter = toks // nx, width // nx
    hz = nz // 2
    bf16, f32 = jnp.bfloat16, jnp.float32
    share = p.expert_gate.shape[2]
    hid = p.dense_gate.shape[0]
    channels = p.conv_state.shape[3]
    state_dim = p.scan_state.shape[3]

    def tall(a):
        return a.reshape(-1, LANES)

    g = SimpleNamespace(**vars(p))
    g.mix_gain, g.post_gain, g.ffn_gain = tall(p.mix_gain), tall(p.post_gain), tall(p.ffn_gain)
    g.dense_switch, g.inner_gain = tall(p.dense_switch), tall(p.inner_gain)
    g.out_gain = tall(p.out_gain)
    g.proj_step, g.expert_router = p.proj_step.T, p.expert_router.T
    g.group_router, g.route_experts = p.group_router.T, p.route_experts.T
    g.resid = p.resid.reshape(nx, own, width)
    g.conv_state = p.conv_state.transpose(1, 2, 0, 3)
    g.scan_state = p.scan_state.reshape(toks, channels, state_dim)
    g.step_bias, g.decay_rate = p.step_bias.reshape(1, -1), p.decay_rate.reshape(1, -1)
    g.expert_gate = p.expert_gate.reshape(nx, quarter, share)
    g.expert_up = p.expert_up.reshape(nx, quarter, share)
    g.expert_down = p.expert_down.reshape(share, width)
    names = tuple(vars(g))
    operands = list(vars(g).values())
    s = SimpleNamespace(**{k: pltpu.VMEM(v.shape, v.dtype) for k, v in vars(g).items()})
    s.dense_gate = s.dense_up = s.dense_down = pltpu.VMEM((np_, hid, quarter), bf16)
    s.expert_down = pltpu.VMEM((nx, share, quarter), bf16)
    s.proj_x = s.proj_b = s.proj_c = s.proj_z = pltpu.VMEM((8, LANES), f32)
    s.proj = pltpu.VMEM((width, 4 * channels), bf16)
    s.fresh = pltpu.VMEM((3, toks, channels), bf16)
    state_rows = (p.scan_state.shape[1] + 1, toks, channels)
    s.rows_ref = pltpu.VMEM(state_rows, f32)
    s.cols_ref = pltpu.VMEM((channels, channels), f32)
    s.c_ref = s.old_read = pltpu.VMEM((toks, channels), f32)
    s.mixed_f = pltpu.VMEM((nx, own, width), f32)
    s.mixed_b = pltpu.VMEM((nx, own, width), bf16)
    s.mixed_in = pltpu.VMEM((nx - 1, own, width), bf16)
    s.feed_out = s.feed_in = pltpu.VMEM((nx, own, quarter), bf16)
    s.stream_out = s.stream_in = pltpu.VMEM((nx, own, quarter), bf16)
    s.pick_in = pltpu.VMEM((nx, own, LANES), f32)
    s.pick_z = pltpu.VMEM((nz, toks, LANES), f32)
    s.code_z = pltpu.VMEM((nz, toks, LANES), bf16)
    s.feed_z = pltpu.VMEM((nz, toks, quarter), bf16)
    s.rows_out = s.rows_in = pltpu.VMEM((2, np_, hz * cap, quarter), bf16)
    s.back_out = s.back_in = pltpu.VMEM((2, np_, hz * cap, quarter), bf16)
    s.rows_x = pltpu.VMEM((2, 3, np_, hz * cap, quarter), bf16)
    s.pre_out = pltpu.VMEM((2, nx, hz * own, 2 * np_ * hid), bf16)
    s.pre_in = pltpu.VMEM((2, nx - 1, hz * own, 2 * np_ * hid), bf16)
    s.hidden_x = pltpu.VMEM((2, nx, hz * own, np_ * hid), bf16)
    s.sum_out = s.sum_in = pltpu.VMEM((2, 6, np_ * hz * cap // 2, quarter), bf16)
    s.last_out = pltpu.VMEM((nz, toks, quarter), bf16)
    s.last_in = pltpu.VMEM((nz, toks, quarter), bf16)
    s.square_x = pltpu.VMEM((nx, 8, LANES), f32)
    plan = names, tuple(vars(s))
    copies = copies_of(nz, np_, nx)
    shapes = [
        pltpu.SemaphoreType.DMA((copies,)),
        pltpu.SemaphoreType.DMA((copies,)),
        pltpu.SemaphoreType.DMA((len(names) + nx + 2,)),
        *vars(s).values(),
    ]
    anyw = pl.BlockSpec(memory_space=pl.ANY)
    return pl.pallas_call(
        functools.partial(layer, sizes, plan),
        out_shape=(
            jax.ShapeDtypeStruct((toks, quarter), bf16),
            jax.ShapeDtypeStruct(state_rows, f32),
            jax.ShapeDtypeStruct((channels, channels), f32),
            jax.ShapeDtypeStruct((3, toks, channels), bf16),
        ),
        in_specs=[anyw] * len(operands),
        out_specs=(pl.BlockSpec(memory_space=pltpu.VMEM), anyw, anyw, anyw),
        scratch_shapes=shapes,
        compiler_params=pltpu.CompilerParams(
            collective_id=0, has_side_effects=True, vmem_limit_bytes=56 * 1024 * 1024
        ),
        name="layer",
    )(*operands)


def finish_step(
    rows_in,
    cols_in,
    fresh_in,
    conv,
    result,
    state,
    new_state,
    new_conv,
    layer_out,
    rows,
    cols,
    fresh,
    conv_v,
    result_v,
    state_v,
    sem,
):
    used = [0]

    def move(src, dst):
        copy = pltpu.make_async_copy(src, dst, sem.at[used[0]])
        used[0] += 1
        copy.start()
        return copy

    toks = state.shape[0]
    heads = rows.shape[0] - 1
    block = 8
    pieces = [pl.ds(i, block) for i in range(0, toks, block)]
    small = [move(rows_in, rows), move(cols_in, cols)]
    states = [move(state.at[at], state_v.at[at]) for at in pieces]
    others = [move(result, result_v), move(conv, conv_v), move(fresh_in, fresh)]
    for copy in small:
        copy.wait()
    head_dim = cols.shape[0] // heads
    out = []
    for i, at in enumerate(pieces):
        states[i].wait()
        for t in range(i * block, (i + 1) * block):
            new = slice(t, t + 1)
            for h in range(heads):
                part = slice(h * head_dim, (h + 1) * head_dim)
                added = cols[part, new] * rows[heads, new]
                state_v[t, part] = rows[h, new] * state_v[t, part] + added
        out.append(move(state_v.at[at], new_state.at[at]))
        if i == 0:
            for copy in others:
                copy.wait()
            out.append(move(result_v, layer_out))
            for k in range(3):
                out.append(move(conv_v.at[k, pl.ds(1, 2)], new_conv.at[k, pl.ds(0, 2)]))
                out.append(move(fresh.at[k], new_conv.at[k, 2]))
    for copy in out:
        copy.wait()


def finish(result, rows, cols, fresh, p):
    toks, heads, head_dim, state_dim = p.scan_state.shape
    channels = heads * head_dim
    conv = p.conv_state.transpose(1, 2, 0, 3)
    state = p.scan_state.reshape(toks, channels, state_dim)
    anyw = pl.BlockSpec(memory_space=pl.ANY)
    operands = (rows, cols, fresh, conv, result, state)
    new_state, new_conv, layer_out = pl.pallas_call(
        finish_step,
        out_shape=tuple(jax.ShapeDtypeStruct(a.shape, a.dtype) for a in (state, conv, result)),
        in_specs=[anyw] * 6,
        out_specs=(anyw,) * 3,
        scratch_shapes=[pltpu.VMEM(a.shape, a.dtype) for a in operands]
        + [pltpu.SemaphoreType.DMA((5 + 2 * (toks // 8) + 7,))],
        name="finish",
    )(*operands)
    return (
        layer_out,
        new_state.reshape(p.scan_state.shape),
        new_conv.transpose(2, 0, 1, 3),
    )


def on_device(
    resid,
    mix_gain,
    proj_x,
    proj_z,
    proj_b,
    proj_c,
    proj_step,
    step_bias,
    decay_rate,
    conv_taps,
    conv_state,
    scan_state,
    inner_gain,
    proj_out,
    post_gain,
    ffn_gain,
    group_router,
    expert_router,
    route_experts,
    expert_gate,
    expert_up,
    expert_down,
    dense_switch,
    dense_gate,
    dense_up,
    dense_down,
    out_gain,
):
    params = SimpleNamespace(**locals())
    sizes = tuple(lax.axis_size(a) for a in EP) + (lax.axis_size("tp"), CAPACITY)
    return finish(*run_layer(sizes, params), params)


TORUS = (8, 4, 2)


def solution(mesh):
    torus = Mesh(mesh.devices.reshape(*TORUS, mesh.shape["tp"]), EP + ("tp",))
    in_specs = (
        P(EP, None),
        P(),
        P(None, "tp"),
        P(None, "tp"),
        P(None, "tp"),
        P(None, "tp"),
        P(),
        P("tp"),
        P("tp"),
        P(None, None, "tp"),
        P(EP, None, None, "tp"),
        P(EP, "tp", None, None),
        P("tp"),
        P("tp", None),
        P(),
        P(),
        P(),
        P(),
        P(EP, None),
        P(EP, None, "tp"),
        P(EP, None, "tp"),
        P(EP, "tp", None),
        P(),
        P(EP, "tp"),
        P(EP, "tp"),
        P(EP, "tp"),
        P("tp"),
    )
    out_specs = (P(EP, "tp"), P(EP, "tp", None, None), P(EP, None, None, "tp"))
    return jax.shard_map(
        on_device, mesh=torus, in_specs=in_specs, out_specs=out_specs, check_vma=False
    )
```

time: 76.4 us -> 72.4 us (0.948)
  Pallas kernels: 75.6 us -> 71.5 us
    pallas_call x1, Pallas kernels: 71.1 us -> 68.2 us  [run_layer(): pl.pallas_call(functools.partial(layer, sizes, plan), out_shape=(jax.Shap...]
    pallas_call x1, Pallas kernels: 4.48 us -> 3.22 us  [finish(): pl.pallas_call(finish_step, out_shape=tuple((jax.ShapeDtypeStruct(a.shape...]
where the time goes in v3:
time: 72.4 us; the launch traced here: 72.1 us
  Pallas kernels  71.5 us (99%)
    pallas_call x1, Pallas kernels, run_layer(): pl.pallas_call(functools.partial(layer, sizes, plan), out_shape=(jax.Shap...  68.2 us
    pallas_call x1, Pallas kernels, finish(): pl.pallas_call(finish_step, out_shape=tuple((jax.ShapeDtypeStruct(a.shape...  3.22 us

profile of v3, /device:TPU:8, one launch (start us, length us, event | category | flops | bytes accessed | tf_op | source)
XLA Modules:
  0.0 72.1 jit_solution(8888400725868685918)
XLA Ops:
  0.6 68.2 %layer.1 = (bf16[32,512]{1,0:T(8,128)(2,1)}, f32[3,32,128]{2,1,0:T(8,128)}, f32[128,128]{1,0:T(8,128)}, bf16[3,32,128]{2,1,0:T(8,128)(2,1)}) custom-call(bf16[4,8,2048]{2,1,0:T(8,128)(2,1)} %bitcast.28, bf16[16,128]{1,0:T(8,128)(2,1)} %bitcast.31, bf16[2048,128]{1,0:T(8,128)(2,1)} %refs_2_.1, bf16[2048,128]{1,0:T(8,128)(2,1)} %refs_3_.1, ...), custom_call_target="tpu_custom_call" | custom-call | tf_op jit(solution)/shard_map/layer/pallas_call | solution.py:642
  68.9 3.2 %finish.1 = (f32[32,128,128]{2,1,0:T(8,128)}, bf16[3,3,32,128]{3,2,1,0:T(8,128)(2,1)}, bf16[32,512]{1,0:T(8,128)(2,1)}) custom-call(f32[3,32,128]{2,1,0:T(8,128)} %get-tuple-element.10.rows_in, f32[128,128]{1,0:T(8,128)} %get-tuple-element.11.cols_in, bf16[3,32,128]{2,1,0:T(8,128)(2,1)} %get-tuple-element.12.fresh_in, bf16[3,3,32,128]{3,2,1,0:T(8,128)(2,1)} %bitcast.26, ...), custom_call_target="tpu_custom_call" | custom-call | tf_op jit(solution)/shard_map/finish/pallas_call | solution.py:724

commit v4 on v3

--- a/solution.py
+++ b/solution.py
@@ -77,35 +77,57 @@
     def x_dev(r):
         return {"tp": lax.rem(x + r, nx)}
 
-    used = [0]
-    started = []
-
-    def send(src, dst, device):
-        k = used[0]
-        used[0] += 1
-        copy = pltpu.make_async_remote_copy(
-            src_ref=src,
-            dst_ref=dst,
-            send_sem=send_sem.at[k],
-            recv_sem=recv_sem.at[k],
-            device_id=device,
-            device_id_type=MESH,
-        )
-        copy.start()
-        started.append(copy)
-        return copy
+    used = SimpleNamespace(send=0, recv=0)
+    at_end = []
+
+    def take_of(whole, sem):
+        return lambda: pltpu.make_async_copy(whole, whole, sem).wait()
+
+    class Group:
+        def __init__(self, whole):
+            self.out_sem, self.in_sem = send_sem.at[used.send], recv_sem.at[used.recv]
+            used.send += 1
+            used.recv += 1
+            self.arrived = take_of(whole, self.in_sem)
+            at_end.append(take_of(whole, self.out_sem))
+
+        def start(self, src, dst, device, in_sem=None):
+            pltpu.make_async_remote_copy(
+                src_ref=src,
+                dst_ref=dst,
+                send_sem=self.out_sem,
+                recv_sem=self.in_sem if in_sem is None else in_sem,
+                device_id=device,
+                device_id_type=MESH,
+            ).start()
+
+    def send(copies, whole, apart=False):
+        if not copies:
+            return []
+        group = Group(whole)
+        waits = []
+        for k, (src, dst, device) in enumerate(copies):
+            in_sem = group.in_sem
+            if apart and k:
+                in_sem = recv_sem.at[used.recv]
+                used.recv += 1
+            group.start(src, dst, device, in_sem)
+            waits.append(take_of(dst, in_sem))
+        return waits if apart else [group.arrived]
 
     local_used = [0]
 
-    def fetch(src, dst):
-        copy = pltpu.make_async_copy(src, dst, local_sem.at[local_used[0]])
-        local_used[0] += 1
+    def fetch(src, dst, sem=None):
+        if sem is None:
+            sem = local_sem.at[local_used[0]]
+            local_used[0] += 1
+        copy = pltpu.make_async_copy(src, dst, sem)
         copy.start()
         return copy
 
-    def arrive(copies):
-        for copy in copies:
-            copy.wait_recv()
+    def arrive(waits):
+        for wait in waits:
+            wait()
 
     barrier = pltpu.get_barrier_semaphore()
     peers = (
@@ -131,12 +153,10 @@
     ready.resid = bring((g.resid, s.resid))
     ready.mix_gain = bring((g.mix_gain, s.mix_gain))
     wide = g.proj_x.shape[1]
-    ready.proj = bring(
-        *(
-            (one, s.proj.at[:, pl.ds(k * wide, wide)])
-            for k, one in enumerate((g.proj_x, g.proj_b, g.proj_c, g.proj_z))
-        )
-    )
+    proj_sem = local_sem.at[local_used[0]]
+    local_used[0] += 1
+    for k, one in enumerate((g.proj_x, g.proj_b, g.proj_c, g.proj_z)):
+        fetch(one, s.proj.at[:, pl.ds(k * wide, wide)], proj_sem)
     ready.proj_step = bring((g.proj_step, s.proj_step))
     ready.conv_taps = bring((g.conv_taps, s.conv_taps))
     ready.conv_state = bring((g.conv_state, s.conv_state))
@@ -156,9 +176,10 @@
     ready.dense_down = bring((g.dense_down, s.dense_down.at[0]))
     ready.expert_gate = bring((g.expert_gate, s.expert_gate))
     ready.expert_up = bring((g.expert_up, s.expert_up))
-    ready.expert_down = bring(
-        *((g.expert_down.at[:, pl.ds(j * quarter, quarter)], s.expert_down.at[j]) for j in range(nx))
-    )
+    down_sem = local_sem.at[local_used[0]]
+    local_used[0] += 1
+    for j in range(nx):
+        fetch(g.expert_down.at[:, pl.ds(j * quarter, quarter)], s.expert_down.at[j], down_sem)
 
     route_t = ready.route_experts()[...]
     picks = route_t.shape[0]
@@ -177,7 +198,7 @@
     gain = in_row(ready.mix_gain())
     normed = root_mean(resid[...].astype(jnp.float32).reshape(toks, width)) * gain
     normed = normed.astype(jnp.bfloat16)
-    ready.proj()
+    take_of(s.proj, proj_sem)()
     projected = dot(normed, s.proj[...])
     step_all = dot_nt(normed, ready.proj_step()[...])
     taps = ready.conv_taps()[...].astype(jnp.float32)
@@ -244,17 +265,24 @@
 
     pl.semaphore_wait(barrier, len(peers))
 
-    copies = [
-        send(mixed_b.at[lax.rem(x + r, nx)], mixed_in.at[r - 1], x_dev(r)) for r in range(1, nx)
-    ]
-    code_copies = [send(code_z.at[here], code_z.at[k], z_dev(order[k])) for k in others]
+    copies = send(
+        [(mixed_b.at[lax.rem(x + r, nx)], mixed_in.at[r - 1], x_dev(r)) for r in range(1, nx)],
+        mixed_in,
+    )
+    code_copies = send(
+        [(code_z.at[here], code_z.at[k], z_dev(order[k])) for k in others],
+        code_z.at[pl.ds(0, nz - 1)],
+    )
     dense_copies = []
     for one, all_here in (
         (g.dense_gate, s.dense_gate),
         (g.dense_up, s.dense_up),
         (g.dense_down, s.dense_down),
     ):
-        dense_copies += [send(one, all_here.at[q], p_dev(q)) for q in range(1, np_)]
+        dense_copies += send(
+            [(one, all_here.at[q], p_dev(q)) for q in range(1, np_)],
+            all_here.at[pl.ds(1, np_ - 1)],
+        )
 
     post_gain, ffn_gain = in_row(ready.post_gain()), in_row(ready.ffn_gain())
     resid_own = resid[x].astype(jnp.float32)
@@ -268,10 +296,18 @@
     stream_out, stream_in = s.stream_out, s.stream_in
     for j in range(nx):
         feed_out[j] = feed[:, j * quarter : (j + 1) * quarter]
+    far = lax.rem(x + 2, nx)
+    far_in = s.far_in
     feed_in[x] = feed_out[x]
-    feed_copies = [
-        send(feed_out.at[lax.rem(x + r, nx)], feed_in.at[x], x_dev(r)) for r in range(1, nx)
-    ]
+    far_in[x] = feed_out[far]
+    feed_copies = send(
+        [(feed_out.at[lax.rem(x + r, nx)], feed_in.at[x], x_dev(r)) for r in range(1, nx)],
+        feed_in.at[pl.ds(0, nx - 1)],
+    )
+    far_copies = send(
+        [(feed_out.at[lax.rem(x + r + 2, nx)], far_in.at[x], x_dev(r)) for r in range(1, nx)],
+        far_in.at[pl.ds(0, nx - 1)],
+    )
     for j in range(nx):
         stream_out[j] = stream[:, j * quarter : (j + 1) * quarter]
 
@@ -313,14 +349,27 @@
     pick_in[x] = pick_table
 
     arrive(feed_copies)
-    feed_z = s.feed_z
+    feed_z, far_z = s.feed_z, s.far_z
     feed_z[here] = feed_in[...].astype(jnp.float32).reshape(toks, quarter).astype(jnp.bfloat16)
-    feed_copies = [send(feed_z.at[here], feed_z.at[k], z_dev(order[k])) for k in others]
-    pick_copies = [send(pick_in.at[x], pick_in.at[x], x_dev(r)) for r in range(1, nx)]
+
+    def to_z(ref, ks):
+        return send(
+            [(ref.at[here], ref.at[k], z_dev(order[k])) for k in ks], ref.at[pl.ds(0, len(ks))]
+        )
+
+    feed_copies = [to_z(feed_z, others[:hz]), to_z(feed_z, others[hz:])]
+    arrive(far_copies)
+    far_z[here] = far_in[...].astype(jnp.float32).reshape(toks, quarter).astype(jnp.bfloat16)
+    far_copies = to_z(far_z, others)
+    pick_copies = send(
+        [(pick_in.at[x], pick_in.at[x], x_dev(r)) for r in range(1, nx)],
+        pick_in.at[pl.ds(0, nx - 1)],
+    )
     stream_in[x] = stream_out[x]
-    stream_copies = [
-        send(stream_out.at[lax.rem(x + r, nx)], stream_in.at[x], x_dev(r)) for r in range(1, nx)
-    ]
+    stream_copies = send(
+        [(stream_out.at[lax.rem(x + r, nx)], stream_in.at[x], x_dev(r)) for r in range(1, nx)],
+        stream_in.at[pl.ds(0, nx - 1)],
+    )
 
     def expert_of(j):
         return z * np_ + ((place + (j >> shift_of(chunk))) & (np_ - 1))
@@ -352,23 +401,41 @@
 
     arrive(pick_copies)
     pick_z[here] = pick_in[...].reshape(toks, LANES)
-    pick_copies = [send(pick_z.at[here], pick_z.at[k], z_dev(order[k])) for k in others]
+    pick_copies = to_z(pick_z, others)
 
     rows_out, rows_in, rows_x = s.rows_out, s.rows_in, s.rows_x
+    far_out = s.far_out
     pre_out, pre_in, hidden_x = s.pre_out, s.pre_in, s.hidden_x
     hidden_here = s.dense_gate.shape[0] * s.dense_gate.shape[1]
     row_copies, pre_copies = [], []
-    from_left, from_right, from_far = ([], []), ([], []), ([], [])
+    to_right, to_left = x_dev(1), x_dev(nx - 1)
+    from_left, from_right, from_far = [], [], []
 
     def rows_to_experts(h):
-        arrive(feed_copies[h * hz : (h + 1) * hz])
+        arrive(feed_copies[h])
         feeds = feed_z[h * hz : (h + 1) * hz].reshape(half_toks, quarter)
         rows_out[h] = dot(put[h], feeds).astype(jnp.bfloat16).reshape(np_, chunk, quarter)
         rows_in[h, 0] = rows_out[h, 0]
         row_copies.append(
-            [None] + [send(rows_out.at[h, q], rows_in.at[h, q], p_dev(q)) for q in range(1, np_)]
+            send(
+                [(rows_out.at[h, q], rows_in.at[h, q], p_dev(q)) for q in range(1, np_)],
+                rows_in.at[h, pl.ds(1, np_ - 1)],
+                apart=True,
+            )
         )
         return feeds
+
+    def far_to_experts(h):
+        feeds = far_z[h * hz : (h + 1) * hz].reshape(half_toks, quarter)
+        value = dot(put[h], feeds).astype(jnp.bfloat16).reshape(np_, chunk, quarter)
+        far_out[h] = value
+        rows_x[h, 2, 0] = far_out[h, 0]
+        from_far.append(
+            send(
+                [(far_out.at[h, q], rows_x.at[h, 2, q], p_dev(q)) for q in range(1, np_)],
+                rows_x.at[h, 2, pl.ds(1, np_ - 1)],
+            )
+        )
 
     def dense_sums(h, feeds):
         ready.dense_gate()
@@ -379,26 +446,25 @@
             part = part.reshape(nx, hz * own, hidden_here).astype(jnp.bfloat16)
             pre_out[h, :, :, k * hidden_here : (k + 1) * hidden_here] = part
         pre_copies.append(
-            [
-                send(pre_out.at[h, lax.rem(x + r, nx)], pre_in.at[h, r - 1], x_dev(r))
-                for r in range(1, nx)
-            ]
+            send(
+                [
+                    (pre_out.at[h, lax.rem(x + r, nx)], pre_in.at[h, r - 1], x_dev(r))
+                    for r in range(1, nx)
+                ],
+                pre_in.at[h],
+            )
         )
 
     def rows_over_x(h):
+        right_group = Group(rows_x.at[h, 0])
+        left_group = Group(rows_x.at[h, 1])
         for q in range(np_):
             if q:
-                row_copies[h][q].wait_recv()
-            from_left[h].append(send(rows_in.at[h, q], rows_x.at[h, 0, q], x_dev(1)))
-            from_right[h].append(send(rows_in.at[h, q], rows_x.at[h, 1, q], x_dev(nx - 1)))
-
-    def pass_on(h):
-        for q in range(half):
-            from_left[h][q].wait_recv()
-            from_far[h].append(send(rows_x.at[h, 0, q], rows_x.at[h, 2, q], x_dev(1)))
-            k = half + q
-            from_right[h][k].wait_recv()
-            from_far[h].append(send(rows_x.at[h, 1, k], rows_x.at[h, 2, k], x_dev(nx - 1)))
+                row_copies[h][q - 1]()
+            right_group.start(rows_in.at[h, q], rows_x.at[h, 0, q], to_right)
+            left_group.start(rows_in.at[h, q], rows_x.at[h, 1, q], to_left)
+        from_left.append([right_group.arrived])
+        from_right.append([left_group.arrived])
 
     w_gate, w_up, w_down = s.expert_gate, s.expert_up, s.expert_down
 
@@ -406,14 +472,14 @@
         taken = taken.reshape(rows, quarter)
         return dot(taken, w_gate[share]), dot(taken, w_up[share])
 
-    right, left, far = lax.rem(x + 1, nx), lax.rem(x + nx - 1, nx), lax.rem(x + 2, nx)
+    right, left = lax.rem(x + 1, nx), lax.rem(x + nx - 1, nx)
 
     def expert_hidden(h):
         gate_value, up_value = of_share(rows_in[h], x)
-        arrive(from_left[h][half:])
+        arrive(from_left[h])
         more = of_share(rows_x[h, 0], left)
         gate_value, up_value = gate_value + more[0], up_value + more[1]
-        arrive(from_right[h][:half])
+        arrive(from_right[h])
         more = of_share(rows_x[h, 1], right)
         gate_value, up_value = gate_value + more[0], up_value + more[1]
         arrive(from_far[h])
@@ -422,12 +488,11 @@
         return (jax.nn.silu(gate_value) * up_value).astype(jnp.bfloat16)
 
     sum_out, sum_in = s.sum_out, s.sum_in
-    to_right, to_left = x_dev(1), x_dev(nx - 1)
     cut = rows // 2
 
     def put_out(h, k, values, device):
         sum_out[h, k] = values.astype(jnp.bfloat16)
-        return send(sum_out.at[h, k], sum_in.at[h, k], device)
+        return send([(sum_out.at[h, k], sum_in.at[h, k], device)], sum_in.at[h, k])
 
     def sums_start(h, hidden):
         low, high = hidden[:cut], hidden[cut:]
@@ -441,32 +506,28 @@
     def sums_pass_on(h, hidden, sums):
         low, high = hidden[:cut], hidden[cut:]
         value = dot(low, w_down[right])
-        sums[0].wait_recv()
+        arrive(sums[0])
         sums.append(put_out(h, 4, value + sum_in[h, 0].astype(jnp.float32), to_right))
         value = dot(high, w_down[left])
-        sums[1].wait_recv()
+        arrive(sums[1])
         sums.append(put_out(h, 5, value + sum_in[h, 1].astype(jnp.float32), to_left))
 
     back_out, back_in = s.back_out, s.back_in
 
     def sums_end(h, hidden, sums):
         done = dot(hidden, w_down[x])
-        back = [None]
         for k, (a, b) in enumerate(((3, 4), (2, 5))):
-            sums[a].wait_recv()
-            sums[b].wait_recv()
+            arrive(sums[a] + sums[b])
             total = done[k * cut : (k + 1) * cut]
             total += sum_in[h, a].astype(jnp.float32) + sum_in[h, b].astype(jnp.float32)
             back_out[h, k * half : (k + 1) * half] = total.astype(jnp.bfloat16).reshape(
                 half, chunk, quarter
             )
-            if k == 0:
-                back_in[h, 0] = back_out[h, 0]
-            back += [
-                send(back_out.at[h, q], back_in.at[h, q], p_dev(np_ - q))
-                for q in range(max(1, k * half), (k + 1) * half)
-            ]
-        return back[1:]
+        back_in[h, 0] = back_out[h, 0]
+        return send(
+            [(back_out.at[h, q], back_in.at[h, q], p_dev(np_ - q)) for q in range(1, np_)],
+            back_in.at[h, pl.ds(1, np_ - 1)],
+        )
 
     def dense_hidden(h):
         arrive(pre_copies[h])
@@ -475,7 +536,10 @@
             pre += pre_in[h, r - 1].astype(jnp.float32)
         value = jax.nn.silu(pre[:, :hidden_here]) * pre[:, hidden_here:]
         hidden_x[h, x] = value.astype(jnp.bfloat16)
-        return [send(hidden_x.at[h, x], hidden_x.at[h, x], x_dev(r)) for r in range(1, nx)]
+        return send(
+            [(hidden_x.at[h, x], hidden_x.at[h, x], x_dev(r)) for r in range(1, nx)],
+            hidden_x.at[h, pl.ds(0, nx - 1)],
+        )
 
     feeds = rows_to_experts(0)
     arrive(dense_copies)
@@ -483,19 +547,20 @@
     feeds = rows_to_experts(1)
     dense_sums(1, feeds)
     rows_over_x(0)
-    pass_on(0)
+    arrive(far_copies)
+    far_to_experts(0)
+    far_to_experts(1)
     rows_over_x(1)
     hidden_copies = [dense_hidden(0)]
     ready.expert_gate()
     ready.expert_up()
-    ready.expert_down()
+    take_of(s.expert_down, down_sem)()
     hidden0 = expert_hidden(0)
     sums0 = sums_start(0, hidden0)
-    pass_on(1)
+    hidden1 = expert_hidden(1)
+    sums1 = sums_start(1, hidden1)
     sums_pass_on(0, hidden0, sums0)
     hidden_copies.append(dense_hidden(1))
-    hidden1 = expert_hidden(1)
-    sums1 = sums_start(1, hidden1)
     backs = [sums_end(0, hidden0, sums0)]
     sums_pass_on(1, hidden1, sums1)
 
@@ -529,9 +594,12 @@
         results = back_in[h].reshape(rows, quarter)
         part = dot(take[h][0], results) + dot(take[h][1], results) + dense_part[h]
         last_out[h * hz : (h + 1) * hz] = part.astype(jnp.bfloat16).reshape(hz, toks, quarter)
-        last.extend(
-            send(last_out.at[k], last_in.at[k], z_dev(nz - order[k]))
-            for k in others[h * hz : (h + 1) * hz]
+        ks = others[h * hz : (h + 1) * hz]
+        last.append(
+            send(
+                [(last_out.at[k], last_in.at[k], z_dev(nz - order[k])) for k in ks],
+                last_in.at[pl.ds(0, len(ks))],
+            )
         )
         return part
 
@@ -541,16 +609,20 @@
     gain = in_row(ready.out_gain())
     arrive(stream_copies)
     stream_part = stream_in[...].astype(jnp.float32).reshape(toks, quarter)
-    for k in others:
-        last[k].wait_recv()
-        combined += last_in[k].astype(jnp.float32)
+    for h in range(2):
+        arrive(last[h])
+        for k in others[h * hz : (h + 1) * hz]:
+            combined += last_in[k].astype(jnp.float32)
 
     square_x = s.square_x
     square = jnp.sum(combined * combined, axis=1, keepdims=True)
     on_lane = iota((toks, LANES), 0) == iota((toks, LANES), 1)
     as_row = jnp.sum(jnp.where(on_lane, square, 0.0), axis=0, keepdims=True)
     square_x[0] = jnp.broadcast_to(as_row, square_x.shape[1:])
-    square_copies = [send(square_x.at[0], square_x.at[r], x_dev(r)) for r in range(1, nx)]
+    square_copies = send(
+        [(square_x.at[0], square_x.at[r], x_dev(r)) for r in range(1, nx)],
+        square_x.at[pl.ds(1, nx - 1)],
+    )
     combined = combined * gain
     arrive(square_copies)
     all_rows = square_x[0]
@@ -560,15 +632,9 @@
     scale = lax.rsqrt(total_square / width + norm_eps)
     layer_out[...] = (stream_part + combined * scale).astype(jnp.bfloat16)
 
-    for copy in started:
-        copy.wait_send()
+    arrive(at_end)
     for copy in small_out:
         copy.wait()
-
-
-def copies_of(nz, np_, nx):
-    x_copies = 6 * (nx - 1) + 4 * (nx - 1) + 4 * np_ + 2 * np_ + 12
-    return x_copies + 4 * (nz - 1) + 7 * (np_ - 1)
 
 
 def run_layer(sizes, p):
@@ -614,13 +680,13 @@
     s.mixed_f = pltpu.VMEM((nx, own, width), f32)
     s.mixed_b = pltpu.VMEM((nx, own, width), bf16)
     s.mixed_in = pltpu.VMEM((nx - 1, own, width), bf16)
-    s.feed_out = s.feed_in = pltpu.VMEM((nx, own, quarter), bf16)
+    s.feed_out = s.feed_in = s.far_in = pltpu.VMEM((nx, own, quarter), bf16)
     s.stream_out = s.stream_in = pltpu.VMEM((nx, own, quarter), bf16)
     s.pick_in = pltpu.VMEM((nx, own, LANES), f32)
     s.pick_z = pltpu.VMEM((nz, toks, LANES), f32)
     s.code_z = pltpu.VMEM((nz, toks, LANES), bf16)
-    s.feed_z = pltpu.VMEM((nz, toks, quarter), bf16)
-    s.rows_out = s.rows_in = pltpu.VMEM((2, np_, hz * cap, quarter), bf16)
+    s.feed_z = s.far_z = pltpu.VMEM((nz, toks, quarter), bf16)
+    s.rows_out = s.rows_in = s.far_out = pltpu.VMEM((2, np_, hz * cap, quarter), bf16)
     s.back_out = s.back_in = pltpu.VMEM((2, np_, hz * cap, quarter), bf16)
     s.rows_x = pltpu.VMEM((2, 3, np_, hz * cap, quarter), bf16)
     s.pre_out = pltpu.VMEM((2, nx, hz * own, 2 * np_ * hid), bf16)
@@ -631,11 +697,11 @@
     s.last_in = pltpu.VMEM((nz, toks, quarter), bf16)
     s.square_x = pltpu.VMEM((nx, 8, LANES), f32)
     plan = names, tuple(vars(s))
-    copies = copies_of(nz, np_, nx)
+    groups = 44
     shapes = [
-        pltpu.SemaphoreType.DMA((copies,)),
-        pltpu.SemaphoreType.DMA((copies,)),
-        pltpu.SemaphoreType.DMA((len(names) + nx + 2,)),
+        pltpu.SemaphoreType.DMA((groups,)),
+        pltpu.SemaphoreType.DMA((groups + 2 * (np_ - 2),)),
+        pltpu.SemaphoreType.DMA((len(names),)),
         *vars(s).values(),
     ]
     anyw = pl.BlockSpec(memory_space=pl.ANY)

time: 72.4 us -> 67.9 us (0.938)
  Pallas kernels: 71.5 us -> 66.8 us
    pallas_call x1, Pallas kernels: 68.2 us -> 63.6 us  [run_layer(): pl.pallas_call(functools.partial(layer, sizes, plan), out_shape=(jax.Shap...]
where the time goes in v4:
time: 67.9 us; the launch traced here: 67.5 us
  Pallas kernels  66.8 us (98%)
    pallas_call x1, Pallas kernels, run_layer(): pl.pallas_call(functools.partial(layer, sizes, plan), out_shape=(jax.Shap...  63.6 us
    pallas_call x1, Pallas kernels, finish(): pl.pallas_call(finish_step, out_shape=tuple((jax.ShapeDtypeStruct(a.shape...  3.22 us

profile of v4, /device:TPU:8, one launch (start us, length us, event | category | flops | bytes accessed | tf_op | source)
XLA Modules:
  0.0 67.5 jit_solution(11406971149971696031)
XLA Ops:
  0.6 63.6 %layer.1 = (bf16[32,512]{1,0:T(8,128)(2,1)}, f32[3,32,128]{2,1,0:T(8,128)}, f32[128,128]{1,0:T(8,128)}, bf16[3,32,128]{2,1,0:T(8,128)(2,1)}) custom-call(bf16[4,8,2048]{2,1,0:T(8,128)(2,1)} %bitcast.28, bf16[16,128]{1,0:T(8,128)(2,1)} %bitcast.31, bf16[2048,128]{1,0:T(8,128)(2,1)} %refs_2_.1, bf16[2048,128]{1,0:T(8,128)(2,1)} %refs_3_.1, ...), custom_call_target="tpu_custom_call" | custom-call | tf_op jit(solution)/shard_map/layer/pallas_call | solution.py:708
  64.3 3.2 %finish.1 = (f32[32,128,128]{2,1,0:T(8,128)}, bf16[3,3,32,128]{3,2,1,0:T(8,128)(2,1)}, bf16[32,512]{1,0:T(8,128)(2,1)}) custom-call(f32[3,32,128]{2,1,0:T(8,128)} %get-tuple-element.10.rows_in, f32[128,128]{1,0:T(8,128)} %get-tuple-element.11.cols_in, bf16[3,32,128]{2,1,0:T(8,128)(2,1)} %get-tuple-element.12.fresh_in, bf16[3,3,32,128]{3,2,1,0:T(8,128)(2,1)} %bitcast.26, ...), custom_call_target="tpu_custom_call" | custom-call | tf_op jit(solution)/shard_map/finish/pallas_call | solution.py:790

commit v5 on v4

--- a/solution.py
+++ b/solution.py
@@ -551,7 +551,6 @@
     far_to_experts(0)
     far_to_experts(1)
     rows_over_x(1)
-    hidden_copies = [dense_hidden(0)]
     ready.expert_gate()
     ready.expert_up()
     take_of(s.expert_down, down_sem)()
@@ -560,16 +559,12 @@
     hidden1 = expert_hidden(1)
     sums1 = sums_start(1, hidden1)
     sums_pass_on(0, hidden0, sums0)
-    hidden_copies.append(dense_hidden(1))
-    backs = [sums_end(0, hidden0, sums0)]
     sums_pass_on(1, hidden1, sums1)
-
+    hidden_copies = [dense_hidden(0), dense_hidden(1)]
     arrive(pick_copies)
     j_col = iota((half_toks, rows), 1)
     same_block = block_of(j_col) == iota((half_toks, rows), 0) >> shift_of(toks)
-    take, dense_part = [], []
-    ready.dense_down()
-    down = s.dense_down[...].reshape(hidden_here, quarter)
+    take, tables = [], []
     for h in range(2):
         table = pick_z[h * hz : (h + 1) * hz].reshape(half_toks, LANES)
         table_hi = table.astype(jnp.bfloat16)
@@ -581,10 +576,17 @@
                 for k in (table_hi, table_lo)
             ]
         )
+        tables.append(table[:, experts : experts + 1])
+
+    backs = [sums_end(0, hidden0, sums0), sums_end(1, hidden1, sums1)]
+    ready.dense_down()
+    down = s.dense_down[...].reshape(hidden_here, quarter)
+    dense_part = []
+    for h in range(2):
         arrive(hidden_copies[h])
         value = hidden_x[h].astype(jnp.float32).reshape(nx, hz, own, hidden_here)
         value = value.swapaxes(0, 1).reshape(half_toks, hidden_here).astype(jnp.bfloat16)
-        dense_part.append(dot(value, down) * table[:, experts : experts + 1])
+        dense_part.append(dot(value, down) * tables[h])
 
     last_out, last_in = s.last_out, s.last_in
     last, parts = [], []
@@ -604,7 +606,6 @@
         return part
 
     give_back(0)
-    backs.append(sums_end(1, hidden1, sums1))
     combined = give_back(1)[(here - hz) * toks : (here - hz + 1) * toks]
     gain = in_row(ready.out_gain())
     arrive(stream_copies)
@@ -708,10 +709,10 @@
     return pl.pallas_call(
         functools.partial(layer, sizes, plan),
         out_shape=(
-            jax.ShapeDtypeStruct((toks, quarter), bf16),
-            jax.ShapeDtypeStruct(state_rows, f32),
-            jax.ShapeDtypeStruct((channels, channels), f32),
-            jax.ShapeDtypeStruct((3, toks, channels), bf16),
+            pltpu.VMEM((toks, quarter), bf16),
+            pltpu.VMEM(state_rows, f32),
+            pltpu.VMEM((channels, channels), f32),
+            pltpu.VMEM((3, toks, channels), bf16),
         ),
         in_specs=[anyw] * len(operands),
         out_specs=(pl.BlockSpec(memory_space=pltpu.VMEM), anyw, anyw, anyw),
@@ -724,22 +725,7 @@
 
 
 def finish_step(
-    rows_in,
-    cols_in,
-    fresh_in,
-    conv,
-    result,
-    state,
-    new_state,
-    new_conv,
-    layer_out,
-    rows,
-    cols,
-    fresh,
-    conv_v,
-    result_v,
-    state_v,
-    sem,
+    rows, cols, fresh, conv, result, state, new_state, new_conv, layer_out, state_v, sem
 ):
     used = [0]
 
@@ -751,31 +737,21 @@
 
     toks = state.shape[0]
     heads = rows.shape[0] - 1
-    block = 8
-    pieces = [pl.ds(i, block) for i in range(0, toks, block)]
-    small = [move(rows_in, rows), move(cols_in, cols)]
-    states = [move(state.at[at], state_v.at[at]) for at in pieces]
-    others = [move(result, result_v), move(conv, conv_v), move(fresh_in, fresh)]
-    for copy in small:
-        copy.wait()
     head_dim = cols.shape[0] // heads
-    out = []
-    for i, at in enumerate(pieces):
-        states[i].wait()
-        for t in range(i * block, (i + 1) * block):
+    block = 4
+    out = [
+        move(result, layer_out),
+        move(conv.at[:, pl.ds(1, 2)], new_conv.at[:, pl.ds(0, 2)]),
+        move(fresh, new_conv.at[:, 2]),
+    ]
+    for i in range(0, toks, block):
+        for t in range(i, i + block):
             new = slice(t, t + 1)
             for h in range(heads):
                 part = slice(h * head_dim, (h + 1) * head_dim)
                 added = cols[part, new] * rows[heads, new]
-                state_v[t, part] = rows[h, new] * state_v[t, part] + added
-        out.append(move(state_v.at[at], new_state.at[at]))
-        if i == 0:
-            for copy in others:
-                copy.wait()
-            out.append(move(result_v, layer_out))
-            for k in range(3):
-                out.append(move(conv_v.at[k, pl.ds(1, 2)], new_conv.at[k, pl.ds(0, 2)]))
-                out.append(move(fresh.at[k], new_conv.at[k, 2]))
+                state_v[t, part] = rows[h, new] * state[t, part] + added
+        out.append(move(state_v.at[pl.ds(i, block)], new_state.at[pl.ds(i, block)]))
     for copy in out:
         copy.wait()
 
@@ -786,16 +762,19 @@
     conv = p.conv_state.transpose(1, 2, 0, 3)
     state = p.scan_state.reshape(toks, channels, state_dim)
     anyw = pl.BlockSpec(memory_space=pl.ANY)
-    operands = (rows, cols, fresh, conv, result, state)
+    vmem = pl.BlockSpec(memory_space=pltpu.VMEM)
     new_state, new_conv, layer_out = pl.pallas_call(
         finish_step,
         out_shape=tuple(jax.ShapeDtypeStruct(a.shape, a.dtype) for a in (state, conv, result)),
-        in_specs=[anyw] * 6,
+        in_specs=[vmem] * 6,
         out_specs=(anyw,) * 3,
-        scratch_shapes=[pltpu.VMEM(a.shape, a.dtype) for a in operands]
-        + [pltpu.SemaphoreType.DMA((5 + 2 * (toks // 8) + 7,))],
+        scratch_shapes=[
+            pltpu.VMEM(state.shape, state.dtype),
+            pltpu.SemaphoreType.DMA((3 + toks // 4,)),
+        ],
+        compiler_params=pltpu.CompilerParams(vmem_limit_bytes=8 * 1024 * 1024),
         name="finish",
-    )(*operands)
+    )(rows, cols, fresh, conv, result, state)
     return (
         layer_out,
         new_state.reshape(p.scan_state.shape),

time: 67.9 us -> 65.2 us (0.960)
  Pallas kernels: 66.8 us -> 64.4 us
    pallas_call x1, Pallas kernels: 3.22 us -> 1.55 us  [finish(): pl.pallas_call(finish_step, out_shape=tuple((jax.ShapeDtypeStruct(a.shape...]
    pallas_call x1, Pallas kernels: 63.6 us -> 62.9 us  [run_layer(): pl.pallas_call(functools.partial(layer, sizes, plan), out_shape=(pltpu.VM...]
where the time goes in v5:
time: 65.2 us; the launch traced here: 65.1 us
  Pallas kernels  64.4 us (99%)
  between operations  0.68 us (1%)
    pallas_call x1, Pallas kernels, run_layer(): pl.pallas_call(functools.partial(layer, sizes, plan), out_shape=(pltpu.VM...  62.9 us
    pallas_call x1, Pallas kernels, finish(): pl.pallas_call(finish_step, out_shape=tuple((jax.ShapeDtypeStruct(a.shape...  1.55 us

profile of v5, /device:TPU:8, one launch (start us, length us, event | category | flops | bytes accessed | tf_op | source)
XLA Modules:
  0.0 65.1 jit_solution(4807673279081315613)
XLA Ops:
  0.6 0.0 copy-start
  0.6 0.0 copy-start.1
  0.7 62.9 %layer.1 = (bf16[32,512]{1,0:T(8,128)(2,1)S(1)}, f32[3,32,128]{2,1,0:T(8,128)S(1)}, f32[128,128]{1,0:T(8,128)S(1)}, bf16[3,32,128]{2,1,0:T(8,128)(2,1)S(1)}) custom-call(bf16[4,8,2048]{2,1,0:T(8,128)(2,1)} %bitcast.28, bf16[16,128]{1,0:T(8,128)(2,1)} %bitcast.31, bf16[2048,128]{1,0:T(8,128)(2,1)} %refs_2_.1, bf16[2048,128]{1,0:T(8,128)(2,1)} %refs_3_.1, ...), custom_call_target="tpu_custom_call" | custom-call | tf_op jit(solution)/shard_map/layer/pallas_call | solution.py:709
  63.5 0.0 copy-done
  63.5 0.0 copy-done.1
  63.5 1.5 %finish.1 = (f32[32,128,128]{2,1,0:T(8,128)}, bf16[3,3,32,128]{3,2,1,0:T(8,128)(2,1)}, bf16[32,512]{1,0:T(8,128)(2,1)}) custom-call(f32[3,32,128]{2,1,0:T(8,128)S(1)} %get-tuple-element.10.rows, f32[128,128]{1,0:T(8,128)S(1)} %get-tuple-element.11.cols, bf16[3,32,128]{2,1,0:T(8,128)(2,1)S(1)} %get-tuple-element.12.fresh, ...), custom_call_target="tpu_custom_call" | custom-call | tf_op jit(solution)/shard_map/finish/pallas_call | solution.py:766
Async XLA Ops:
  0.6 62.9 %copy-start = (f32[32,2,64,128]{3,2,1,0:T(8,128)S(1)}, f32[32,2,64,128]{3,2,1,0:T(8,128)}, u32[]{:S(2)}) copy-start(f32[32,2,64,128]{3,2,1,0:T(8,128)} %param.38) | copy-start | bytes 6291460
  0.6 62.9 %copy-start.1 = (bf16[32,3,3,128]{3,0,2,1:T(8,128)(2,1)S(1)}, bf16[32,3,3,128]{3,0,2,1:T(8,128)(2,1)}, u32[]{:S(2)}) copy-start(bf16[32,3,3,128]{3,0,2,1:T(8,128)(2,1)} %param.37) | copy-start | bytes 221188

commit v6 on v5

--- a/solution.py
+++ b/solution.py
@@ -273,17 +273,6 @@
         [(code_z.at[here], code_z.at[k], z_dev(order[k])) for k in others],
         code_z.at[pl.ds(0, nz - 1)],
     )
-    dense_copies = []
-    for one, all_here in (
-        (g.dense_gate, s.dense_gate),
-        (g.dense_up, s.dense_up),
-        (g.dense_down, s.dense_down),
-    ):
-        dense_copies += send(
-            [(one, all_here.at[q], p_dev(q)) for q in range(1, np_)],
-            all_here.at[pl.ds(1, np_ - 1)],
-        )
-
     post_gain, ffn_gain = in_row(ready.post_gain()), in_row(ready.ffn_gain())
     resid_own = resid[x].astype(jnp.float32)
     arrive(copies)
@@ -308,6 +297,16 @@
         [(feed_out.at[lax.rem(x + r + 2, nx)], far_in.at[x], x_dev(r)) for r in range(1, nx)],
         far_in.at[pl.ds(0, nx - 1)],
     )
+    dense_copies = []
+    for one, all_here in (
+        (g.dense_gate, s.dense_gate),
+        (g.dense_up, s.dense_up),
+        (g.dense_down, s.dense_down),
+    ):
+        dense_copies += send(
+            [(one, all_here.at[q], p_dev(q)) for q in range(1, np_)],
+            all_here.at[pl.ds(1, np_ - 1)],
+        )
     for j in range(nx):
         stream_out[j] = stream[:, j * quarter : (j + 1) * quarter]
 

time: 65.2 us -> 65.9 us (1.011); the launches traced: 65.1 us -> 65.1 us
  no operation moved by 1% of the time
where the time goes in v6:
time: 65.9 us; the launch traced here: 65.1 us
  Pallas kernels  64.4 us (98%)
  between operations  0.68 us (1%)
    pallas_call x1, Pallas kernels, run_layer(): pl.pallas_call(functools.partial(layer, sizes, plan), out_shape=(pltpu.VM...  62.9 us
    pallas_call x1, Pallas kernels, finish(): pl.pallas_call(finish_step, out_shape=tuple((jax.ShapeDtypeStruct(a.shape...  1.55 us

profile of v6, /device:TPU:8, one launch (start us, length us, event | category | flops | bytes accessed | tf_op | source)
XLA Modules:
  0.0 65.1 jit_solution(4273619881295513659)
XLA Ops:
  0.6 0.0 copy-start
  0.6 0.0 copy-start.1
  0.7 62.9 %layer.1 = (bf16[32,512]{1,0:T(8,128)(2,1)S(1)}, f32[3,32,128]{2,1,0:T(8,128)S(1)}, f32[128,128]{1,0:T(8,128)S(1)}, bf16[3,32,128]{2,1,0:T(8,128)(2,1)S(1)}) custom-call(bf16[4,8,2048]{2,1,0:T(8,128)(2,1)} %bitcast.28, bf16[16,128]{1,0:T(8,128)(2,1)} %bitcast.31, bf16[2048,128]{1,0:T(8,128)(2,1)} %refs_2_.1, bf16[2048,128]{1,0:T(8,128)(2,1)} %refs_3_.1, ...), custom_call_target="tpu_custom_call" | custom-call | tf_op jit(solution)/shard_map/layer/pallas_call | solution.py:708
  63.6 0.0 copy-done
  63.6 0.0 copy-done.1
  63.6 1.5 %finish.1 = (f32[32,128,128]{2,1,0:T(8,128)}, bf16[3,3,32,128]{3,2,1,0:T(8,128)(2,1)}, bf16[32,512]{1,0:T(8,128)(2,1)}) custom-call(f32[3,32,128]{2,1,0:T(8,128)S(1)} %get-tuple-element.10.rows, f32[128,128]{1,0:T(8,128)S(1)} %get-tuple-element.11.cols, bf16[3,32,128]{2,1,0:T(8,128)(2,1)S(1)} %get-tuple-element.12.fresh, ...), custom_call_target="tpu_custom_call" | custom-call | tf_op jit(solution)/shard_map/finish/pallas_call | solution.py:765
Async XLA Ops:
  0.6 62.9 %copy-start = (f32[32,2,64,128]{3,2,1,0:T(8,128)S(1)}, f32[32,2,64,128]{3,2,1,0:T(8,128)}, u32[]{:S(2)}) copy-start(f32[32,2,64,128]{3,2,1,0:T(8,128)} %param.38) | copy-start | bytes 6291460
  0.6 62.9 %copy-start.1 = (bf16[32,3,3,128]{3,0,2,1:T(8,128)(2,1)S(1)}, bf16[32,3,3,128]{3,0,2,1:T(8,128)(2,1)}, u32[]{:S(2)}) copy-start(bf16[32,3,3,128]{3,0,2,1:T(8,128)(2,1)} %param.37) | copy-start | bytes 221188
